TPU v7x, 256 devices: a whole 4x4x8 slice. The times are simulated.
256 devices in a mesh: ep: 16 (over y, x), tp: 16 (over z, core).
Axes of the slice: x: 4, y: 4, z: 8, core: 2. Of those that a mesh axis runs over, the one named last changes fastest.
Arguments:
- queries: bfloat16 [12288, 2048], P('ep', 'tp'), may hold values from -6 to 6
- values: bfloat16 [12288, 2048], P('ep', 'tp'), may hold values from -6 to 6
- forget_gate_logits: bfloat16 [2, 12288, 2048], P(None, 'ep', 'tp'), may hold values from -5 to 5
- output_gate_logits: bfloat16 [12288, 2048], P('ep', 'tp'), may hold values from -6 to 6
- forget_gate_headroom: float32 [2, 2048], P(None, 'tp'), may hold values from 0 to 0.1, as said below
- spike_log_decay: float32 [12288], P('ep'), may hold values from -1.6 to 0
- head_norm_gain: float32 [2048], P('tp'), may hold values from 0.1 to 1.9
- output_projection: bfloat16 [2048, 2048], P(None, 'tp'), may hold values from -0.125 to 0.125
- second_micro_input: bfloat16 [12288, 2048], P('ep'), may hold values from -170 to 170
- expert_norm_gain: float32 [2048], replicated, may hold values from 0.1 to 1.9
- token_group_index: int32 [12288], P('ep'), may hold values from 0 to 7, as said below
- token_expert_pair: int32 [12288, 2], P('ep'), may hold values from 0 to 3, as said below
- group_router_scores: float32 [12288, 8], P('ep'), may hold values from -6 to 320
- expert_router_scores: float32 [12288, 2], P('ep'), may hold values from -6 to 6
- expert_gate_weight: bfloat16 [32, 2048, 4096], P('ep', None, 'tp'), may hold values from -0.125 to 0.125
- expert_up_weight: bfloat16 [32, 2048, 4096], P('ep', None, 'tp'), may hold values from -0.125 to 0.125
- expert_down_weight: bfloat16 [32, 4096, 2048], P('ep', 'tp'), may hold values from -1.25 to 1.25
Outputs:
- recurrence_output: bfloat16 [12288, 2048], P('ep', 'tp')
- expert_tokens: bfloat16 [12288, 2048], P('ep', 'tp')
Inputs may be any that keep to these rules, and one draw needn't show every extreme that they name: `token_group_index`: within the rows of one device each of the 8 groups is named by the same number of rows. The two entries of a row differ. Within the rows of one device every expert token_group_index * 4 + token_expert_pair is named exactly 48 times. `forget_gate_headroom`: Positive.
All inputs are finite; a program needn't handle non-finite values.
Results may differ from a plain program's by a relative error of at most 0.018.
Values may be sent and summed in bfloat16 or wider, within the bound.
A program may use at most 128 MiB of HBM per device.

v0:
```python
import jax
import jax.numpy as jnp
from jax import lax
from jax.sharding import Mesh
from jax.sharding import PartitionSpec as P

HEAD_DIM = 128
GROUP_EXP = 4
BLOCK = 64
TP = ("tp_0", "tp_1")


HEAD_EPS = 1e-06
NORM_EPS = 1e-05


def from_everyone(value, axis):
    copies = jnp.broadcast_to(value, (lax.axis_size(axis), *value.shape))
    return lax.all_to_all(copies, axis, split_axis=0, concat_axis=0, tiled=True)


def collected_together(value, axis):
    leaves = jax.tree.leaves(value)
    order = sorted(range(len(leaves)), key=lambda k: -leaves[k].size)
    width = (1, *leaves[order[0]].shape)[-1]
    lines = [
        jnp.pad(leaves[k].reshape(-1), (0, -leaves[k].size % width)).reshape(-1, width)
        for k in order
    ]
    both, at, found = (from_everyone(jnp.concatenate(lines), axis), 0, {})
    for k, line in zip(order, lines):
        piece = both[:, at : at + len(line)].reshape(len(both), -1)
        found[k] = piece[:, : leaves[k].size].reshape(-1, *leaves[k].shape)
        at += len(line)
    numbers = iter(range(len(leaves)))
    return jax.tree.map(lambda _: found[next(numbers)], value)


def joined_by_halves(pieces, combine):
    while len(jax.tree.leaves(pieces)[0]) > 1:
        pieces = jax.vmap(combine)(
            *(jax.tree.map(lambda part: part[side::2], pieces) for side in (0, 1))
        )
    return jax.tree.map(lambda part: part[0], pieces)


def prefix(value, axis, combine, identity, reverse):
    count, place = (lax.axis_size(axis), lax.axis_index(axis))
    passed = jnp.arange(count) > place if reverse else jnp.arange(count) < place

    def kept(part, zero, own):
        part = jnp.where(
            passed.reshape(-1, *(1 for _ in own.shape)),
            part.astype(own.dtype),
            jnp.asarray(zero, own.dtype),
        )
        return part[::-1] if reverse else part

    pieces = collected_together(
        jax.tree.map(lambda part, kind: part.astype(kind), value, (jnp.bfloat16, jnp.bfloat16)),
        axis,
    )
    return joined_by_halves(jax.tree.map(kept, pieces, identity, value), combine)


def scatter_axes(value, axes, dim):
    for axis in axes:
        value = lax.psum_scatter(value, axis, scatter_dimension=dim, tiled=True)
    return value


def decay_pieces(forget_gate_logits, forget_gate_headroom, spike_log_decay):
    logits = forget_gate_logits.astype(jnp.float32)
    gap_span = forget_gate_headroom[:, None, :]
    logarithm_decay = jnp.logaddexp(
        jnp.log1p(-gap_span), jnp.log(gap_span) + jax.nn.log_sigmoid(logits)
    )
    logarithm_decay = logarithm_decay + spike_log_decay[None, :, None]
    key_contributions = gap_span * jax.nn.sigmoid(-logits)
    return (logarithm_decay, key_contributions)


def combine_states(earlier, following):
    return (earlier[0] + following[0], jnp.exp(following[0])[..., None] * earlier[1] + following[1])


def on_device(
    queries,
    values,
    forget_gate_logits,
    output_gate_logits,
    forget_gate_headroom,
    spike_log_decay,
    head_norm_gain,
    output_projection,
    second_micro_input,
    expert_norm_gain,
    token_group_index,
    token_expert_pair,
    group_router_scores,
    expert_router_scores,
    expert_gate_weight,
    expert_up_weight,
    expert_down_weight,
):
    row_count = queries.shape[0]
    head_count = forget_gate_headroom.shape[1] // HEAD_DIM
    block_count = row_count // BLOCK
    logarithm_decay, key_contributions = decay_pieces(
        forget_gate_logits, forget_gate_headroom, spike_log_decay
    )
    lifted = jax.nn.silu(queries.astype(jnp.float32))
    inputs_f = values.astype(jnp.float32)

    def directed(tensor):
        both = jnp.stack([tensor[0], jnp.flip(tensor[1], 0)])
        return both.reshape(2, block_count, BLOCK, head_count, HEAD_DIM)

    query_dir = directed(jnp.stack([lifted, lifted]))
    value_dir = directed(jnp.stack([inputs_f, inputs_f]))
    key_dir = directed(key_contributions)
    running_state = jnp.cumsum(directed(logarithm_decay), axis=2)
    final_block_row = running_state[:, :, -1:]
    query_up = query_dir * jnp.exp(running_state - final_block_row)
    key_down = key_dir * jnp.exp(final_block_row - running_state)
    scores = jnp.einsum("nbthk,nbshk->nbhts", query_up, key_down)
    causal = jnp.tril(jnp.ones((BLOCK, BLOCK), bool))
    scores = jnp.where(causal, scores, 0.0)
    inner_out = jnp.einsum("nbhts,nbshv->nbthv", scores, value_dir)
    block_states = jnp.einsum("nbshk,nbshv->nbhkv", key_down, value_dir)
    block_decay = final_block_row[:, :, 0]
    through = jnp.cumsum(block_decay, axis=1)
    entry_sum = through - block_decay
    block_ids = jnp.arange(block_count)
    earlier_mask = (block_ids[None, :] < block_ids[:, None])[None, :, :, None, None]
    between = entry_sum[:, :, None] - through[:, None, :]
    carry_wts = jnp.where(earlier_mask, jnp.exp(jnp.where(earlier_mask, between, 0.0)), 0.0)
    local_entry = jnp.einsum("nbchk,nchkv->nbhkv", carry_wts, block_states)
    device_decay = through[:, -1]
    tail_wts = jnp.exp(device_decay[:, None] - through)
    device_state = jnp.einsum("nchk,nchkv->nhkv", tail_wts, block_states)
    zero_decay = jnp.zeros_like(device_decay[0])
    zero_state = jnp.zeros_like(device_state[0])
    forward_pair = prefix(
        (device_decay[0], device_state[0]), "ep", combine_states, (zero_decay, zero_state), False
    )
    backward_pair = prefix(
        (device_decay[1], device_state[1]), "ep", combine_states, (zero_decay, zero_state), True
    )
    incoming = jnp.stack([forward_pair[1], backward_pair[1]])
    block_entry = local_entry + jnp.exp(entry_sum)[..., None] * incoming[:, None]
    across_block_output = jnp.einsum(
        "nbthk,nbhkv->nbthv", query_dir * jnp.exp(running_state), block_entry
    )
    direction_out = (across_block_output + inner_out).reshape(2, row_count, head_count, HEAD_DIM)
    joined = direction_out[0] + jnp.flip(direction_out[1], 0)
    normed = joined * lax.rsqrt(jnp.mean(joined * joined, -1, keepdims=True) + HEAD_EPS)
    readout = (
        normed.reshape(row_count, -1)
        * head_norm_gain
        * jax.nn.silu(output_gate_logits.astype(jnp.float32))
    ).astype(jnp.bfloat16)
    mixed_sum = jnp.dot(
        lax.all_gather(readout, TP, axis=1, tiled=True),
        output_projection,
        preferred_element_type=jnp.float32,
    )
    recurrence_output = mixed_sum.astype(jnp.bfloat16)
    features = second_micro_input.astype(jnp.float32)
    centred = features - jnp.mean(features, -1, keepdims=True)
    normed_input = (
        centred
        * lax.rsqrt(jnp.mean(centred * centred, -1, keepdims=True) + NORM_EPS)
        * expert_norm_gain
    ).astype(jnp.bfloat16)
    group_count = group_router_scores.shape[1]
    group_prob = jax.nn.softmax(group_router_scores, axis=-1)
    chosen = jnp.sum(
        jnp.where(jnp.arange(group_count)[None, :] == token_group_index[:, None], group_prob, 0.0),
        -1,
    )
    pair_weight = (
        jnp.stack(
            [
                jax.nn.sigmoid(expert_router_scores[:, 0] - expert_router_scores[:, 1]),
                jax.nn.sigmoid(expert_router_scores[:, 1] - expert_router_scores[:, 0]),
            ],
            -1,
        )
        * chosen[:, None]
    )
    expert_count = group_count * GROUP_EXP
    per_device = expert_gate_weight.shape[0]
    ep_size = lax.axis_size("ep")
    capacity = 2 * row_count // expert_count
    expert_id = (token_group_index[:, None] * GROUP_EXP + token_expert_pair).reshape(-1)
    onehot = (expert_id[:, None] == jnp.arange(expert_count)[None, :]).astype(jnp.int32)
    slot_rank = jnp.sum(onehot * (jnp.cumsum(onehot, axis=0) - 1), axis=1)
    slot_index = expert_id * capacity + slot_rank
    source_row = (
        jnp.zeros((2 * row_count,), jnp.int32)
        .at[slot_index]
        .set(jnp.arange(2 * row_count, dtype=jnp.int32) // 2)
    )
    outgoing = normed_input[source_row].reshape(ep_size, per_device, capacity, -1)
    flat_slots = outgoing.reshape(ep_size, per_device * capacity, -1)
    share_rows = flat_slots.shape[1] // lax.axis_size(TP)
    own_share = lax.dynamic_slice_in_dim(flat_slots, lax.axis_index(TP) * share_rows, share_rows, 1)
    landed = lax.all_to_all(own_share, "ep", split_axis=0, concat_axis=0, tiled=True)
    complete = lax.all_gather(landed, TP, axis=1, tiled=True)
    arrived = complete.reshape(outgoing.shape)
    gate_terms = jnp.einsum(
        "secd,edf->secf", arrived, expert_gate_weight, preferred_element_type=jnp.float32
    )
    up_terms = jnp.einsum(
        "secd,edf->secf", arrived, expert_up_weight, preferred_element_type=jnp.float32
    )
    hidden = (jax.nn.silu(gate_terms) * up_terms).astype(jnp.bfloat16)
    partial_value = jnp.einsum(
        "secf,efd->secd", hidden, expert_down_weight, preferred_element_type=jnp.float32
    )
    summed = (
        scatter_axes(partial_value.astype(jnp.bfloat16), TP, 3)
        .astype(jnp.float32)
        .astype(jnp.bfloat16)
    )
    returned = lax.all_to_all(summed, "ep", split_axis=0, concat_axis=0, tiled=True)
    copies = (
        returned.reshape(2 * row_count, -1)[slot_index]
        .reshape(row_count, 2, -1)
        .astype(jnp.float32)
    )
    expert_tokens = jnp.sum(copies * pair_weight[:, :, None], axis=1).astype(jnp.bfloat16)
    return (recurrence_output, expert_tokens)


def solution(mesh):
    split = Mesh(mesh.devices.reshape(mesh.shape["ep"], 8, 2), ("ep", "tp_0", "tp_1"))
    placed = (
        P("ep", TP),
        P("ep", TP),
        P(None, "ep", TP),
        P("ep", TP),
        P(None, TP),
        P("ep"),
        P(TP),
        P(None, TP),
        P("ep", None),
        P(),
        P("ep"),
        P("ep", None),
        P("ep", None),
        P("ep", None),
        P("ep", None, TP),
        P("ep", None, TP),
        P("ep", TP, None),
    )
    return jax.shard_map(
        on_device,
        mesh=split,
        in_specs=placed,
        out_specs=(P("ep", TP), P("ep", TP)),
        check_vma=False,
    )
```

profile of v0, /device:TPU:4, one launch (start us, length us, event | category | flops | bytes accessed | tf_op | source)
XLA Modules:
  0.0 297.9 jit_solution(9439619995598031195)
XLA Ops:
  7.2 0.8 broadcast_multiply_fusion.1
  8.1 0.7 broadcast_multiply_fusion
  8.8 0.2 copy.92
  8.9 0.2 eq.42
  9.2 0.2 eq.38
  9.4 9.1 %reduce-window.6 = s32[32,12,128]{2,1,0:T(8,128)S(1)} reduce-window(s32[32,12,128]{2,1,0:T(8,128)S(1)} %fusion.93, s32[]{:T(128)} %constant.75.clone.1), window={size=1x1x128 pad=0_0x0_0x127_0}, to_apply=%region_5.6 | reduce-window | flops 6242304 | bytes 393220 | tf_op jit(solution)/shard_map/reduce-window
  18.7 0.2 copy.94
  19.3 0.3 mul.287
  19.7 6.2 %scatter_custom_fusion = s32[1536]{0:T(1024)S(1)} fusion(s32[1536]{0:T(1024)S(1)} %fusion.101, s32[1536]{0:T(1024)S(1)} %add_select_fusion, s32[]{:T(128)} %constant.75.clone.1), kind=kCustom, calls=%fused_computation.161 | custom fusion | bytes 6148 | tf_op jit(solution)/shard_map/scatter | solution.py:203
  25.9 2.5 convert_reduce_fusion
  28.5 0.3 copy-done.2
  28.7 1.0 fusion.2
  29.7 4.6 %fusion.4 = bf16[768,2048]{1,0:T(8,128)(2,1)} fusion(bf16[768,2048]{1,0:T(8,128)(2,1)} %param.25, f32[2048]{0:T(1024)S(1)} %copy-done.18, f32[768]{0:T(1024)S(1)} %add_rsqrt_fusion, f32[768]{0:T(1024)S(1)} %broadcast_multiply_fusion.2), kind=kLoop, calls=%fused_computation.9 | loop fusion | flops 7864320 | bytes 6305792 | tf_op jit(solution)/shard_map/convert_element_type | solution.py:175
  34.3 15.0 %gather_fusion = bf16[1536,2048]{1,0:T(8,128)(2,1)} fusion(bf16[768,2048]{1,0:T(8,128)(2,1)} %fusion.4, s32[2048]{0:T(1024)S(1)} %pad_clamp_fusion.1), kind=kCustom, calls=%fused_computation | custom fusion | bytes 12589056 | tf_op jit(solution)/shard_map/gather | solution.py:205
  49.3 1.4 constant_dynamic-slice_fusion
  50.7 16.2 %all_to_all.20 = bf16[16,6,2048]{2,1,0:T(8,128)(2,1)S(1)} all-to-all(bf16[16,6,2048]{2,1,0:T(8,128)(2,1)S(1)} %constant_dynamic-slice_fusion), channel_id=1, replica_groups=mesh['ep'=16,'tp_0'=8,'tp_1'=2] {'ep'}, dimensions={0} | all-to-all | bytes 786432 | tf_op jit(solution)/shard_map/all_to_all | solution.py:209
  66.8 1.0 copy.96
  67.8 0.2 reduce-scatter.5.cloned.1.call-start
  68.0 47.2 %all-gather.5.cloned.1.call-done = bf16[16,96,2048]{2,0,1:T(8,128)(2,1)} async-done(((bf16[16,6,2048]{2,0,1:T(8,128)(2,1)}), bf16[16,96,2048]{2,0,1:T(8,128)(2,1)}) %all-gather.5.cloned.1.call-update) | async-done | bytes 6291472 | tf_op jit(solution)/shard_map/all_gather | solution.py:210
  115.3 8.7 %fusion.7 = f32[2,16,48,256]{3,2,1,0:T(8,128)} fusion(bf16[16,2,48,2048]{3,0,2,1:T(8,128)(2,1)} %bitcast.200, bf16[2,2048,256]{2,1,0:T(8,128)(2,1)} %param.31), kind=kOutput, calls=%fused_computation.13 | convolution fusion | flops 1610612736 | bytes 9961472 | tf_op jit(solution)/shard_map/secd,edf->secf/dot_general | solution.py:212
  124.0 12.7 %convert_bitcast_fusion = bf16[16,2,48,2048]{3,2,0,1:T(8,128)(2,1)} fusion(bf16[2,256,2048]{2,1,0:T(8,128)(2,1)S(1)} %copy-done, f32[2,16,48,256]{3,2,1,0:T(8,128)} %fusion.7, bf16[2,2048,256]{2,1,0:T(8,128)(2,1)} %param.32, bf16[16,2,48,2048]{3,0,2,1:T(8,128)(2,1)} %bitcast.201), kind=kOutput, calls=%fused_computation.10 | convolution fusion | flops 3226730496 | bytes 18350080 | tf_op jit(solution)/shard_map/secf,efd->secd/dot_general | solution.py:219
  136.7 0.6 copy-done.21
  137.4 0.3 copy-done.9
  137.7 1.1 fusion.66
  139.0 0.4 rev.20
  139.4 0.2 copy.79
  139.6 0.2 copy.78
  140.2 0.2 copy.77
  140.5 0.2 copy.76
  141.0 0.2 rev.21
  141.3 0.8 copy.102
  142.1 0.2 copy_dynamic-update-slice_fusion.1
  142.3 0.2 copy_dynamic-update-slice_fusion
  142.6 1.6 fusion.51
  144.2 0.4 fusion.69
  144.6 0.9 copy-done.5
  145.5 0.6 fusion.9
  146.2 1.0 broadcast_in_dim.120
  147.2 7.3 %all-to-all-start.1 = ((bf16[16,129,128]{2,1,0:T(8,128)(2,1)}), bf16[16,129,128]{2,1,0:T(8,128)(2,1)S(1)}, u32[]{:S(2)}, u32[]{:S(2)}) async-start(bf16[16,129,128]{2,1,0:T(8,128)(2,1)} %broadcast_in_dim.120), calls=%async_computation.1 | async-start | bytes 1114112 | tf_op jit(solution)/shard_map/all_to_all | solution.py:19
  154.5 0.8 copy.81
  155.2 0.8 copy.84
  156.0 0.8 copy.82
  156.8 1.4 fusion.45
  158.3 5.8 %all-to-all-done.1 = bf16[16,129,128]{2,1,0:T(8,128)(2,1)S(1)} async-done(((bf16[16,129,128]{2,1,0:T(8,128)(2,1)}), bf16[16,129,128]{2,1,0:T(8,128)(2,1)S(1)}, u32[]{:S(2)}, u32[]{:S(2)}) %all-to-all-start.1) | async-done | bytes 528416 | tf_op jit(solution)/shard_map/all_to_all | solution.py:19
  164.1 1.0 broadcast_in_dim.115
  165.1 6.1 %all-to-all-start = ((bf16[16,129,128]{2,1,0:T(8,128)(2,1)}), bf16[16,129,128]{2,1,0:T(8,128)(2,1)S(1)}, u32[]{:S(2)}, u32[]{:S(2)}) async-start(bf16[16,129,128]{2,1,0:T(8,128)(2,1)} %broadcast_in_dim.115), calls=%async_computation | async-start | bytes 1114112 | tf_op jit(solution)/shard_map/all_to_all | solution.py:19
  171.3 8.4 %all-to-all-done = bf16[16,129,128]{2,1,0:T(8,128)(2,1)S(1)} async-done(((bf16[16,129,128]{2,1,0:T(8,128)(2,1)}), bf16[16,129,128]{2,1,0:T(8,128)(2,1)S(1)}, u32[]{:S(2)}, u32[]{:S(2)}) %all-to-all-start) | async-done | bytes 528416 | tf_op jit(solution)/shard_map/all_to_all | solution.py:19
  180.1 0.2 slice_add_fusion
  180.9 0.2 reverse_add_fusion
  181.4 29.3 %reduce-scatter.5.cloned.1.call-done = bf16[16,2,48,256]{3,2,0,1:T(8,128)(2,1)} async-done(((bf16[16,2,48,2048]{3,2,0,1:T(8,128)(2,1)}), bf16[16,2,48,256]{3,2,0,1:T(8,128)(2,1)}) %reduce-scatter.5.cloned.1.call-update) | async-done | bytes 786448 | tf_op jit(solution)/shard_map/reduce_scatter | solution.py:68
  210.6 3.9 %copy.109 = bf16[16,2,48,256]{2,0,1,3:T(8,128)(2,1)S(1)} copy(bf16[16,2,48,256]{3,2,0,1:T(8,128)(2,1)} %reduce-scatter.5.cloned.1.call-done) | data formatting | bytes 1572864
  214.5 4.8 %reshape.443 = bf16[256,1536]{1,0:T(8,128)(2,1)} reshape(bf16[256,2,16,48]{3,2,1,0:T(8,128)(2,1)S(1)} %bitcast.173) | data formatting | bytes 1572864
  219.6 3.1 %fusion.16 = bf16[2,12,128,128]{3,1,2,0:T(8,128)(2,1)S(1)} fusion(bf16[2,12,128,128]{3,2,1,0:T(8,128)(2,1)S(1)} %copy-done.6, f32[2,128,128]{2,1,0:T(8,128)S(1)} %maximum_bitcast_fusion.2, f32[2,12,128]{1,2,0:T(8,128)S(1)} %copy-done.14, f32[2,12,128]{1,2,0:T(8,128)S(1)} %copy-done.15, f32[2,12,128]{1,2,0:T(8,128)S(1)} %copy-done.13, ...), kind=kOutput, calls=%fused_computation.24 | convolution fusion | flops 10727424 | bytes 1740944 | tf_op jit(solution)/shard_map/nbchk,nchkv->nbhkv/dot_general | solution.py:138
  222.7 0.3 fusion.42
  223.6 0.9 fusion.91
  224.6 6.9 %reduce-scatter.7.cloned.1.call-done = bf16[128,1536]{1,0:T(8,128)(2,1)} async-done(((bf16[256,1536]{1,0:T(8,128)(2,1)}), bf16[128,1536]{1,0:T(8,128)(2,1)}) %reduce-scatter.7.cloned.1.call-update) | async-done | bytes 393232
  231.6 2.1 reshape.444
  233.7 1.8 copy.100
  235.4 7.3 %all-to-all-start.3 = ((bf16[16,2,48,128]{3,2,1,0:T(8,128)(2,1)}), bf16[16,2,48,128]{3,2,1,0:T(8,128)(2,1)S(1)}, u32[]{:S(2)}, u32[]{:S(2)}) async-start(bf16[16,2,48,128]{3,2,1,0:T(8,128)(2,1)} %copy.100), calls=%async_computation.4 | async-start | bytes 786432 | tf_op jit(solution)/shard_map/all_to_all | solution.py:227
  242.7 0.2 copy.101
  242.9 36.6 %all-gather.3.cloned.1.call-done = bf16[768,2048]{1,0:T(8,128)(2,1)} async-done(((bf16[768,128]{1,0:T(8,128)(2,1)}), bf16[768,2048]{1,0:T(8,128)(2,1)}) %all-gather.3.cloned.1.call-update) | async-done | bytes 3145744 | tf_op jit(solution)/shard_map/all_gather | solution.py:164
  279.5 3.8 %convolution_convert_fusion = bf16[768,128]{1,0:T(8,128)(2,1)} fusion(bf16[768,2048]{1,0:T(8,128)(2,1)} %all-gather.3.cloned.1.call-done, bf16[2048,128]{1,0:T(8,128)(2,1)} %param.24), kind=kOutput, calls=%fused_computation.42 | convolution fusion | flops 402751488 | bytes 3866624 | tf_op jit(solution)/shard_map/dot_general | solution.py:163
  283.3 3.2 %gather_fusion.1 = bf16[1536,128]{1,0:T(8,128)(2,1)S(1)} fusion(bf16[1536,128]{1,0:T(8,128)(2,1)S(1)} %bitcast.172, s32[2048]{0:T(1024)S(1)} %pad_clamp_fusion), kind=kCustom, calls=%fused_computation.1 | custom fusion | bytes 792576 | tf_op jit(solution)/shard_map/gather | solution.py:229
  286.5 4.8 %fusion.75 = bf16[768,128]{1,0:T(8,128)(2,1)} fusion(bf16[768,2,128]{2,1,0:T(2,128)(2,1)S(1)} %bitcast.180, f32[768,2]{1,0:T(8,128)S(1)} %copy.101), kind=kLoop, calls=%fused_computation.82 | loop fusion | flops 491520 | bytes 595968 | tf_op jit(solution)/shard_map/reduce_sum | solution.py:233
  (116 shorter events, 3.7 us)
Async XLA Ops:
  7.2 116.8 %copy-start = (bf16[2,256,2048]{2,1,0:T(8,128)(2,1)S(1)}, bf16[2,256,2048]{2,1,0:T(8,128)(2,1)}, u32[]{:S(2)}) copy-start(bf16[2,256,2048]{2,1,0:T(8,128)(2,1)} %param.33) | copy-start | bytes 6291460
  7.2 108.1 %all-gather.5.cloned.1.call-start = ((), (), s32[]{:S(2)}) async-start(), calls=%async_computation.7 | async-start | bytes 6684672 | tf_op jit(solution)/shard_map/all_gather | solution.py:210
  25.9 2.8 copy-start.2
  25.9 3.8 %copy-start.18 = (f32[2048]{0:T(1024)S(1)}, f32[2048]{0:T(1024)}, u32[]{:S(2)}) copy-start(f32[2048]{0:T(1024)} %param.26) | copy-start | bytes 24580
  67.8 142.8 %reduce-scatter.5.cloned.1.call-start = ((), (), s32[]{:S(2)}) async-start(), calls=%async_computation.8 | async-start | bytes 7077888 | tf_op jit(solution)/shard_map/reduce_scatter | solution.py:68
  136.7 0.7 copy-start.21
  136.7 1.0 copy-start.9
  136.7 1.0 copy-start.20
  139.4 1.4 copy-start.11
  139.9 1.2 copy-start.4
  142.6 2.9 copy-start.16
  144.2 12.7 %copy-start.8 = (bf16[2,12,64,128]{3,1,2,0:T(8,128)(2,1)S(1)}, bf16[2,12,64,128]{3,1,2,0:T(8,128)(2,1)}, u32[]{:S(2)}) copy-start(bf16[2,12,64,128]{3,1,2,0:T(8,128)(2,1)} %get-tuple-element.5) | copy-start | bytes 1179652
  144.6 0.9 copy-start.5
  147.2 16.9 %all-to-all-start.1 = ((bf16[16,129,128]{2,1,0:T(8,128)(2,1)}), bf16[16,129,128]{2,1,0:T(8,128)(2,1)S(1)}, u32[]{:S(2)}, u32[]{:S(2)}) async-start(bf16[16,129,128]{2,1,0:T(8,128)(2,1)} %broadcast_in_dim.120), calls=%async_computation.1 | async-start | bytes 1114112 | tf_op jit(solution)/shard_map/all_to_all | solution.py:19
  165.1 14.7 %all-to-all-start = ((bf16[16,129,128]{2,1,0:T(8,128)(2,1)}), bf16[16,129,128]{2,1,0:T(8,128)(2,1)S(1)}, u32[]{:S(2)}, u32[]{:S(2)}) async-start(bf16[16,129,128]{2,1,0:T(8,128)(2,1)} %broadcast_in_dim.115), calls=%async_computation | async-start | bytes 1114112 | tf_op jit(solution)/shard_map/all_to_all | solution.py:19
  171.2 60.4 %reduce-scatter.7.cloned.1.call-start = ((), (), s32[]{:S(2)}) async-start(), calls=%async_computation.9 | async-start | bytes 1179648
  181.3 38.2 %copy-start.6 = (bf16[2,12,128,128]{3,2,1,0:T(8,128)(2,1)S(1)}, bf16[2,12,128,128]{3,2,1,0:T(8,128)(2,1)}, u32[]{:S(2)}) copy-start(bf16[2,12,128,128]{3,2,1,0:T(8,128)(2,1)} %copy-done.5) | copy-start | bytes 2359300
  181.3 38.2 %copy-start.13 = (f32[2,12,128]{1,2,0:T(8,128)S(1)}, f32[2,12,128]{1,2,0:T(8,128)}, u32[]{:S(2)}) copy-start(f32[2,12,128]{1,2,0:T(8,128)} %copy.81) | copy-start | bytes 36868
  181.4 38.2 %copy-start.14 = (f32[2,12,128]{1,2,0:T(8,128)S(1)}, f32[2,12,128]{1,2,0:T(8,128)}, u32[]{:S(2)}) copy-start(f32[2,12,128]{1,2,0:T(8,128)} %copy.84) | copy-start | bytes 36868
  181.4 38.2 %copy-start.15 = (f32[2,12,128]{1,2,0:T(8,128)S(1)}, f32[2,12,128]{1,2,0:T(8,128)}, u32[]{:S(2)}) copy-start(f32[2,12,128]{1,2,0:T(8,128)} %copy.82) | copy-start | bytes 36868
  219.3 60.2 %all-gather.3.cloned.1.call-start = ((), (), s32[]{:S(2)}) async-start(), calls=%async_computation.6 | async-start | bytes 3342336 | tf_op jit(solution)/shard_map/all_gather | solution.py:164
  219.5 3.1 %copy-start.3 = (bf16[2,12,64,128]{3,1,2,0:T(8,128)(2,1)S(1)}, bf16[2,12,64,128]{3,1,2,0:T(8,128)(2,1)}, u32[]{:S(2)}) copy-start(bf16[2,12,64,128]{3,1,2,0:T(8,128)(2,1)} %get-tuple-element.4) | copy-start | bytes 1179652
  219.6 3.1 %copy-start.7 = (f32[2,12,128,64]{2,3,1,0:T(8,128)S(1)}, f32[2,12,128,64]{2,3,1,0:T(8,128)}, u32[]{:S(2)}) copy-start(f32[2,12,128,64]{2,3,1,0:T(8,128)} %fusion.45) | copy-start | bytes 2359300
  222.7 0.9 copy-start.12
  222.7 0.9 copy-start.22
  222.7 1.8 copy-start.10
  222.7 1.8 copy-start.17
  222.7 1.8 copy-start.19
  235.4 47.9 %all-to-all-start.3 = ((bf16[16,2,48,128]{3,2,1,0:T(8,128)(2,1)}), bf16[16,2,48,128]{3,2,1,0:T(8,128)(2,1)S(1)}, u32[]{:S(2)}, u32[]{:S(2)}) async-start(bf16[16,2,48,128]{3,2,1,0:T(8,128)(2,1)} %copy.100), calls=%async_computation.4 | async-start | bytes 786432 | tf_op jit(solution)/shard_map/all_to_all | solution.py:227
  279.5 11.8 %copy-start.1 = (bf16[2,256,2048]{2,1,0:T(8,128)(2,1)S(1)}, bf16[2,256,2048]{2,1,0:T(8,128)(2,1)}, u32[]{:S(2)}) copy-start(bf16[2,256,2048]{2,1,0:T(8,128)(2,1)} %param.33) | copy-start | bytes 6291460
Sparse Core Ops, SparseCore 0:
  67.9 47.2 all-gather.4
  136.9 73.7 reduce-scatter.4
  219.5 12.0 reduce-scatter.6
  233.7 45.7 all-gather.2
where the time goes:
time: 300 us; the launch traced here: 298 us
  waiting for transfers between devices  134 us (45%)
  local copies, waits for them, and re-layouts  51.1 us (17%)
  matrix products  31.1 us (10%)
  other arithmetic  29.6 us (10%)
  starting transfers between devices  21 us (7%)
  blocking collectives  16.2 us (5%)
  between operations  14.6 us (5%)
    all_gather x1, waiting for transfers between devices, on_device(): complete = lax.all_gather(landed, TP, axis=1, tiled=True)  47.2 us
    all_gather x1, waiting for transfers between devices, on_device(): lax.all_gather(readout, TP, axis=1, tiled=True)  36.6 us
    reduce_scatter x1, waiting for transfers between devices, scatter_axes(): value = lax.psum_scatter(value, axis, scatter_dimension=dim, tiled=True)  29.3 us
    all_to_all x1, blocking collectives, on_device(): lax.all_to_all(own_share, 'ep', split_axis=0, concat_axis=0, tiled=True)  16.2 us
    gather x1, local copies, waits for them, and re-layouts, on_device(): normed_input[source_row].reshape(ep_size, per_device, capacity, -1)  15 us
    all_to_all x2, waiting for transfers between devices, from_everyone(): return lax.all_to_all(copies, axis, split_axis=0, concat_axis=0, tiled=True)  14.3 us
    all_to_all x2, starting transfers between devices, from_everyone(): return lax.all_to_all(copies, axis, split_axis=0, concat_axis=0, tiled=True)  13.4 us
    unnamed x50, local copies, waits for them, and re-layouts  13.3 us
  transfers between devices with their start and end apart: 7, of which 6 were waited for; matrix products, arithmetic and copies ran while one was open for 9% of the time, Pallas kernels for 0%

commit v1 on v0

--- a/solution.py
+++ b/solution.py
@@ -1,6 +1,10 @@
+import functools
+
 import jax
 import jax.numpy as jnp
 from jax import lax
+from jax.experimental import pallas as pl
+from jax.experimental.pallas import tpu as pltpu
 from jax.sharding import Mesh
 from jax.sharding import PartitionSpec as P
 
@@ -63,12 +67,6 @@
     return joined_by_halves(jax.tree.map(kept, pieces, identity, value), combine)
 
 
-def scatter_axes(value, axes, dim):
-    for axis in axes:
-        value = lax.psum_scatter(value, axis, scatter_dimension=dim, tiled=True)
-    return value
-
-
 def decay_pieces(forget_gate_logits, forget_gate_headroom, spike_log_decay):
     logits = forget_gate_logits.astype(jnp.float32)
     gap_span = forget_gate_headroom[:, None, :]
@@ -82,6 +80,334 @@
 
 def combine_states(earlier, following):
     return (earlier[0] + following[0], jnp.exp(following[0])[..., None] * earlier[1] + following[1])
+
+
+F32, BF16 = jnp.float32, jnp.bfloat16
+RINGS = ((0, 0), (0, 1), (1, 0), (1, 1))
+
+
+def mm(a, b):
+    return jnp.dot(a, b, preferred_element_type=F32)
+
+
+def expert_kernel(
+    x_hbm, gain, eid_row, eid_col, weight_col, wg_hbm, wu_hbm, wd_hbm, out,
+    x, normed, wg, wu, wd, rank_row, send_buf, arrived, partial, pair_buf,
+    ring_buf, final_buf, ret, pick0, pick1,
+    load_sem, disp_send, disp_recv, fwd_send, fwd_recv, pair_send, pair_recv,
+    ring_send, ring_recv, ret_send, ret_recv,
+):
+    side = arrived.shape[1]
+    cap = arrived.shape[3]
+    zs = partial.shape[1]
+    rows, width = x.shape
+    group_rows = side * cap
+    ep_size = side * side
+    experts = 2 * ep_size
+    me, z, core = lax.axis_index("ep"), lax.axis_index("tp_0"), lax.axis_index("tp_1")
+    my_y, my_x = me // side, me % side
+    loads = [
+        pltpu.make_async_copy(a, b, load_sem.at[n])
+        for n, (a, b) in enumerate(((x_hbm, x), (wg_hbm, wg), (wu_hbm, wu), (wd_hbm, wd)))
+    ]
+    for load in loads:
+        load.start()
+
+    barrier = pltpu.get_barrier_semaphore()
+
+    def greet(n, carry):
+        pl.semaphore_signal(barrier, 1, device_id={"ep": (me + n) % ep_size})
+        return carry
+
+    lax.fori_loop(1, ep_size, greet, 0)
+    pl.semaphore_signal(barrier, 1, device_id={"tp_1": 1 - core})
+    pl.semaphore_signal(barrier, 1, device_id={"tp_0": (z + 1) % zs})
+    pl.semaphore_signal(barrier, 1, device_id={"tp_0": (z + zs - 1) % zs})
+
+    def target(k, m):
+        return ((my_y + 2 * side - (m + k) % side) % side) * side + (my_x + side - m) % side
+
+    def source(k, m):
+        return ((my_y + (m + k) % side) % side) * side + (my_x + m) % side
+
+    first = lax.broadcasted_iota(jnp.int32, (rows, rows), 0)
+    second = lax.broadcasted_iota(jnp.int32, (rows, rows), 1)
+    ids = lax.broadcasted_iota(jnp.int32, (experts, rows), 0)
+    named = (ids == eid_row[0:1, :]) | (ids == eid_row[1:2, :])
+    before = jnp.where(first < second, 1.0, 0.0).astype(BF16)
+    rank = mm(jnp.where(named, 1.0, 0.0).astype(BF16), before)
+    rank_row[...] = jnp.where(named, rank, -1.0)
+    ids_col = lax.broadcasted_iota(jnp.int32, (rows, experts), 1)
+    is0, is1 = ids_col == eid_col[:, 0:1], ids_col == eid_col[:, 1:2]
+    after = jnp.where(second < first, 1.0, 0.0).astype(BF16)
+    slot = mm(after, jnp.where(is0 | is1, 1.0, 0.0).astype(BF16)) + (cap * ids_col).astype(F32)
+    places = lax.broadcasted_iota(jnp.int32, (rows, pick0.shape[1]), 1).astype(F32)
+    for pick, chosen in ((pick0, is0), (pick1, is1)):
+        where_to = jnp.sum(jnp.where(chosen, slot, 0.0), axis=1, keepdims=True)
+        pick[...] = jnp.where(places == where_to, 1.0, 0.0).astype(BF16)
+
+    loads[0].wait()
+    step_rows = 16
+
+    def norm_step(n, carry):
+        at = pl.ds(pl.multiple_of(n * step_rows, step_rows), step_rows)
+        features = x[at, :].astype(F32)
+        centred = features - jnp.mean(features, -1, keepdims=True)
+        spread = lax.rsqrt(jnp.mean(centred * centred, -1, keepdims=True) + NORM_EPS)
+        normed[at, :] = (centred * spread * gain[...]).astype(BF16)
+        return carry
+
+    lax.fori_loop(0, rows // step_rows, norm_step, 0)
+    pl.semaphore_wait(barrier, ep_size + 2)
+
+    def dispatch_copy(k, m):
+        return pltpu.make_async_remote_copy(
+            send_buf.at[k, m], arrived.at[core, k, m], disp_send.at[k, m], disp_recv.at[k, m],
+            device_id={"ep": target(k, m)},
+        )
+
+    def forward_copy(k, m):
+        return pltpu.make_async_remote_copy(
+            arrived.at[core, k, m], arrived.at[core, k, m], fwd_send.at[k, m], fwd_recv.at[k, m],
+            device_id={"tp_1": 1 - core},
+        )
+
+    places_row = lax.broadcasted_iota(jnp.int32, (cap, rows), 0).astype(F32)
+
+    def gather_group(k, carry):
+        picks = [
+            jnp.where(
+                rank_row[pl.ds(2 * target(k, m) + core, 1), :] == places_row, 1.0, 0.0
+            ).astype(BF16)
+            for m in range(side)
+        ]
+        sel = jnp.concatenate(picks, 0)
+        for n in range(0, width, 512):
+            got = mm(sel, normed[:, n : n + 512]).astype(BF16)
+            send_buf[k, :, :, n : n + 512] = got.reshape(side, cap, 512)
+        for m in range(side):
+            if m == 0:
+                @pl.when(k == 0)
+                def _():
+                    arrived[core, 0, 0] = send_buf[0, 0]
+
+                @pl.when(k > 0)
+                def _():
+                    dispatch_copy(k, m).start()
+            else:
+                dispatch_copy(k, m).start()
+        return carry
+
+    lax.fori_loop(0, side, gather_group, 0)
+    for load in loads[1:]:
+        load.wait()
+
+    def ring_length(h, f):
+        return zs // 2 if h == f else zs // 2 - 1
+
+    def half(h):
+        return pl.ds(h * group_rows, group_rows)
+
+    def neighbour(f):
+        return (z + 1) % zs if f == 0 else (z + zs - 1) % zs
+
+    def ring_copy(k, h, f, s):
+        length = ring_length(h, f)
+        toward = (z + length) % zs if f == 0 else (z + zs - length) % zs
+        origin = partial.at[k, toward, core, half(h)] if s == 0 else ring_buf.at[k, h, f, s - 1]
+        return pltpu.make_async_remote_copy(
+            origin, ring_buf.at[k, h, f, s], ring_send.at[k, h, f, s], ring_recv.at[k, h, f, s],
+            device_id={"tp_0": neighbour(f)},
+        )
+
+    def ring_step(k, s):
+        for h, f in RINGS:
+            length = ring_length(h, f)
+            if s >= length:
+                continue
+            if s > 0:
+                ring_copy(k, h, f, s - 1).wait_recv()
+                left = length - s
+                toward = (z + left) % zs if f == 0 else (z + zs - left) % zs
+                ring_buf[k, h, f, s - 1] = (
+                    ring_buf[k, h, f, s - 1].astype(F32)
+                    + partial[k, toward, core, half(h)].astype(F32)
+                ).astype(BF16)
+            ring_copy(k, h, f, s).start()
+
+    def pair_copy(k):
+        return pltpu.make_async_remote_copy(
+            partial.at[k, :, 1 - core], pair_buf.at[k], pair_send.at[k], pair_recv.at[k],
+            device_id={"tp_1": 1 - core},
+        )
+
+    def return_copy(k, m):
+        return pltpu.make_async_remote_copy(
+            final_buf.at[k, :, m], ret.at[me], ret_send.at[k, m], ret_recv.at[me],
+            device_id={"ep": source(k, m)},
+        )
+
+    def finish(k):
+        for h in range(2):
+            lengths = [ring_length(h, f) for f in range(2)]
+            for f in range(2):
+                ring_copy(k, h, f, lengths[f] - 1).wait_recv()
+            total = (
+                partial[k, z, core, half(h)].astype(F32)
+                + ring_buf[k, h, 0, lengths[0] - 1].astype(F32)
+                + ring_buf[k, h, 1, lengths[1] - 1].astype(F32)
+            )
+            final_buf[k, h] = total.astype(BF16).reshape(final_buf.shape[2:])
+        for m in range(side):
+            if m == 0:
+                @pl.when(k == 0)
+                def _():
+                    ret[me] = final_buf[0, :, 0]
+
+                @pl.when(k > 0)
+                def _():
+                    return_copy(k, m).start()
+            else:
+                return_copy(k, m).start()
+
+    def take_pair(k):
+        pair_copy(k).wait_recv()
+        for d in range(zs):
+            partial[k, d, core] = (
+                partial[k, d, core].astype(F32) + pair_buf[k, d].astype(F32)
+            ).astype(BF16)
+
+    def compute(k):
+        for q in range(2):
+            tokens = arrived[q, k].reshape(group_rows, width)
+            gate = mm(tokens, wg[q])
+            up = mm(tokens, wu[q])
+            hidden = (jax.nn.silu(gate) * up).astype(BF16)
+            for n in range(0, width, 512):
+                part = mm(hidden, wd[q, :, n : n + 512]).astype(BF16)
+                for i in range(4):
+                    s = n // 128 + i
+                    partial[k, s // 2, s % 2, half(q)] = part[:, 128 * i : 128 * i + 128]
+
+    def group_step(k, carry):
+        for m in range(side):
+            if m == 0:
+                @pl.when(k > 0)
+                def _():
+                    dispatch_copy(k, 0).wait_recv()
+            else:
+                dispatch_copy(k, m).wait_recv()
+            forward_copy(k, m).start()
+
+            @pl.when(k > 0)
+            def _():
+                ring_step(k - 1, m)
+
+        for m in range(side):
+            forward_copy(k, m).wait_recv()
+        compute(k)
+        pair_copy(k).start()
+
+        @pl.when(k > 0)
+        def _():
+            finish(k - 1)
+
+        take_pair(k)
+        return carry
+
+    lax.fori_loop(0, side, group_step, 0)
+    for s in range(side):
+        ring_step(side - 1, s)
+    finish(side - 1)
+
+    def take_returns(k, carry):
+        for m in range(side):
+            def wait_one():
+                there = target(k, m)
+                pltpu.make_async_remote_copy(
+                    final_buf.at[k, :, m], ret.at[there], ret_send.at[k, m], ret_recv.at[there],
+                    device_id={"ep": there},
+                ).wait_recv()
+
+            if m == 0:
+                pl.when(k > 0)(wait_one)
+            else:
+                wait_one()
+        return carry
+
+    lax.fori_loop(0, side, take_returns, 0)
+    copies = ret[...].reshape(pick0.shape[1], 128)
+    out[...] = (
+        weight_col[:, 0:1] * mm(pick0[...], copies) + weight_col[:, 1:2] * mm(pick1[...], copies)
+    ).astype(BF16)
+
+    def drain(k, carry):
+        for m in range(side):
+            def sent():
+                dispatch_copy(k, m).wait_send()
+                return_copy(k, m).wait_send()
+
+            if m == 0:
+                pl.when(k > 0)(sent)
+            else:
+                sent()
+            forward_copy(k, m).wait_send()
+        pair_copy(k).wait_send()
+        for h, f in RINGS:
+            for s in range(ring_length(h, f)):
+                ring_copy(k, h, f, s).wait_send()
+        return carry
+
+    lax.fori_loop(0, side, drain, 0)
+
+
+def expert_side(x, gain, eid_row, eid_col, weight_col, wg, wu, wd):
+    rows, width = x.shape
+    ep_size, zs = lax.axis_size("ep"), lax.axis_size("tp_0")
+    side = int(round(ep_size**0.5))
+    experts = 2 * ep_size
+    cap = 2 * rows // experts
+    group_rows = side * cap
+    ring_slots = zs // 2
+    dma = pltpu.SemaphoreType.DMA
+    vmem = pl.BlockSpec(memory_space=pltpu.VMEM)
+    hbm = pl.BlockSpec(memory_space=pl.ANY)
+    return pl.pallas_call(
+        expert_kernel,
+        out_shape=jax.ShapeDtypeStruct((rows, width // (2 * zs)), BF16),
+        in_specs=[hbm, vmem, vmem, vmem, vmem, hbm, hbm, hbm],
+        out_specs=vmem,
+        scratch_shapes=[
+            pltpu.VMEM(x.shape, BF16),
+            pltpu.VMEM(x.shape, BF16),
+            pltpu.VMEM(wg.shape, BF16),
+            pltpu.VMEM(wu.shape, BF16),
+            pltpu.VMEM(wd.shape, BF16),
+            pltpu.VMEM((experts, rows), F32),
+            pltpu.VMEM((side, side, cap, width), BF16),
+            pltpu.VMEM((2, side, side, cap, width), BF16),
+            pltpu.VMEM((side, zs, 2, 2 * group_rows, 128), BF16),
+            pltpu.VMEM((side, zs, 2 * group_rows, 128), BF16),
+            pltpu.VMEM((side, 2, 2, ring_slots, group_rows, 128), BF16),
+            pltpu.VMEM((side, 2, side, cap, 128), BF16),
+            pltpu.VMEM((ep_size, 2, cap, 128), BF16),
+            pltpu.VMEM((rows, experts * cap), BF16),
+            pltpu.VMEM((rows, experts * cap), BF16),
+            dma((4,)),
+            dma((side, side)), dma((side, side)),
+            dma((side, side)), dma((side, side)),
+            dma((side,)), dma((side,)),
+            dma((side, 2, 2, ring_slots)), dma((side, 2, 2, ring_slots)),
+            dma((side, side)), dma((ep_size,)),
+        ],
+        compiler_params=pltpu.CompilerParams(
+            collective_id=0, has_side_effects=True, vmem_limit_bytes=60 * 1024 * 1024
+        ),
+        cost_estimate=pl.CostEstimate(
+            flops=40_000_000_000, bytes_accessed=20_000_000, transcendentals=0
+        ),
+        name="expert_side",
+    )(x, gain, eid_row, eid_col, weight_col, wg, wu, wd)
 
 
 def on_device(
@@ -166,13 +492,6 @@
         preferred_element_type=jnp.float32,
     )
     recurrence_output = mixed_sum.astype(jnp.bfloat16)
-    features = second_micro_input.astype(jnp.float32)
-    centred = features - jnp.mean(features, -1, keepdims=True)
-    normed_input = (
-        centred
-        * lax.rsqrt(jnp.mean(centred * centred, -1, keepdims=True) + NORM_EPS)
-        * expert_norm_gain
-    ).astype(jnp.bfloat16)
     group_count = group_router_scores.shape[1]
     group_prob = jax.nn.softmax(group_router_scores, axis=-1)
     chosen = jnp.sum(
@@ -189,48 +508,17 @@
         )
         * chosen[:, None]
     )
-    expert_count = group_count * GROUP_EXP
-    per_device = expert_gate_weight.shape[0]
-    ep_size = lax.axis_size("ep")
-    capacity = 2 * row_count // expert_count
-    expert_id = (token_group_index[:, None] * GROUP_EXP + token_expert_pair).reshape(-1)
-    onehot = (expert_id[:, None] == jnp.arange(expert_count)[None, :]).astype(jnp.int32)
-    slot_rank = jnp.sum(onehot * (jnp.cumsum(onehot, axis=0) - 1), axis=1)
-    slot_index = expert_id * capacity + slot_rank
-    source_row = (
-        jnp.zeros((2 * row_count,), jnp.int32)
-        .at[slot_index]
-        .set(jnp.arange(2 * row_count, dtype=jnp.int32) // 2)
-    )
-    outgoing = normed_input[source_row].reshape(ep_size, per_device, capacity, -1)
-    flat_slots = outgoing.reshape(ep_size, per_device * capacity, -1)
-    share_rows = flat_slots.shape[1] // lax.axis_size(TP)
-    own_share = lax.dynamic_slice_in_dim(flat_slots, lax.axis_index(TP) * share_rows, share_rows, 1)
-    landed = lax.all_to_all(own_share, "ep", split_axis=0, concat_axis=0, tiled=True)
-    complete = lax.all_gather(landed, TP, axis=1, tiled=True)
-    arrived = complete.reshape(outgoing.shape)
-    gate_terms = jnp.einsum(
-        "secd,edf->secf", arrived, expert_gate_weight, preferred_element_type=jnp.float32
-    )
-    up_terms = jnp.einsum(
-        "secd,edf->secf", arrived, expert_up_weight, preferred_element_type=jnp.float32
-    )
-    hidden = (jax.nn.silu(gate_terms) * up_terms).astype(jnp.bfloat16)
-    partial_value = jnp.einsum(
-        "secf,efd->secd", hidden, expert_down_weight, preferred_element_type=jnp.float32
-    )
-    summed = (
-        scatter_axes(partial_value.astype(jnp.bfloat16), TP, 3)
-        .astype(jnp.float32)
-        .astype(jnp.bfloat16)
-    )
-    returned = lax.all_to_all(summed, "ep", split_axis=0, concat_axis=0, tiled=True)
-    copies = (
-        returned.reshape(2 * row_count, -1)[slot_index]
-        .reshape(row_count, 2, -1)
-        .astype(jnp.float32)
-    )
-    expert_tokens = jnp.sum(copies * pair_weight[:, :, None], axis=1).astype(jnp.bfloat16)
+    expert_id = token_group_index[:, None] * GROUP_EXP + token_expert_pair
+    expert_tokens = expert_side(
+        second_micro_input,
+        expert_norm_gain[None, :],
+        expert_id.T,
+        expert_id,
+        pair_weight,
+        expert_gate_weight,
+        expert_up_weight,
+        expert_down_weight,
+    )
     return (recurrence_output, expert_tokens)
 
 

time: 300 us -> 212 us (0.71)
  Pallas kernels: 0 us -> 123 us
  waiting for transfers between devices: 134 us -> 14 us
  local copies, waits for them, and re-layouts: 51.1 us -> 22.3 us
  matrix products: 31.1 us -> 10.2 us
  other arithmetic: 29.6 us -> 13 us
  blocking collectives: 16.2 us -> 0 us
  starting transfers between devices: 21 us -> 13.8 us
    pallas_call x0 -> x1, Pallas kernels: none -> 123 us  [expert_side(): pl.pallas_call(expert_kernel, out_shape=jax.ShapeDtypeStruct((rows, width...]
    all_gather x1 -> x0, waiting for transfers between devices: 47.2 us -> none  [on_device(): complete = lax.all_gather(landed, TP, axis=1, tiled=True)]
    all_gather x1, waiting for transfers between devices: 36.6 us -> 0.02 us  [on_device(): lax.all_gather(readout, TP, axis=1, tiled=True)]
    reduce_scatter x1 -> x0, waiting for transfers between devices: 29.3 us -> none  [scatter_axes(): value = lax.psum_scatter(value, axis, scatter_dimension=dim, tiled=True)]
    dot_general x2 -> x0, matrix products: 21.4 us -> none  [the longest x1 12.7 us: on_device(): jnp.einsum('secf,efd->secd', hidden, expert_down_weight, preferred_elemen...]
    gather x2 -> x0, local copies, waits for them, and re-layouts: 18.2 us -> none  [the longest x1 15 us: on_device(): normed_input[source_row].reshape(ep_size, per_device, capacity, -1)]
    all_to_all x1 -> x0, blocking collectives: 16.2 us -> none  [on_device(): lax.all_to_all(own_share, 'ep', split_axis=0, concat_axis=0, tiled=True)]
    unnamed x50 -> x53, local copies, waits for them, and re-layouts: 13.3 us -> 3.79 us
  transfers between devices with their start and end apart: 7 -> 3, of which waited for: 6 -> 2; matrix products, arithmetic and copies ran while one was open for 9% -> 3% of each run, Pallas kernels for 0% -> 58%
where the time goes in v1:
time: 212 us; the launch traced here: 211 us
  Pallas kernels  123 us (58%)
  local copies, waits for them, and re-layouts  22.3 us (11%)
  between operations  14.7 us (7%)
  waiting for transfers between devices  14 us (7%)
  starting transfers between devices  13.8 us (7%)
  other arithmetic  13 us (6%)
  matrix products  10.2 us (5%)
    pallas_call x1, Pallas kernels, expert_side(): pl.pallas_call(expert_kernel, out_shape=jax.ShapeDtypeStruct((rows, width...  123 us
    all_to_all x2, waiting for transfers between devices, from_everyone(): return lax.all_to_all(copies, axis, split_axis=0, concat_axis=0, tiled=True)  13.9 us
    all_to_all x2, starting transfers between devices, from_everyone(): return lax.all_to_all(copies, axis, split_axis=0, concat_axis=0, tiled=True)  13.5 us
    rev x4, local copies, waits for them, and re-layouts, directed(): both = jnp.stack([tensor[0], jnp.flip(tensor[1], 0)])  7.9 us
  transfers between devices with their start and end apart: 3, of which 2 were waited for; matrix products, arithmetic and copies ran while one was open for 3% of the time, Pallas kernels for 58%

profile of v1, /device:TPU:4, one launch (start us, length us, event | category | flops | bytes accessed | tf_op | source)
XLA Modules:
  0.0 210.8 jit_solution(8282566542172593234)
XLA Ops:
  7.2 0.7 negate_log-plus-one_fusion
  7.9 2.1 %fusion.42 = (f32[2,768,128]{2,1,0:T(8,128)S(1)}, f32[2,768,128]{2,1,0:T(8,128)S(1)}) fusion(bf16[2,768,128]{2,1,0:T(8,128)(2,1)} %param.19, f32[2,128]{1,0:T(2,128)} %param.21, f32[768]{0:T(1024)} %param.22, f32[2,128]{1,0:T(2,128)S(1)} %get-tuple-element.40, f32[2,128]{1,0:T(2,128)S(1)} %get-tuple-element.39), kind=kLoop, calls=%fused_computation.46 | loop fusion | flops 4325376 | bytes 1972224 | tf_op jit(solution)/shard_map/mul | solution.py:77
  10.1 0.9 fusion.80
  10.9 0.1 rev.20
  11.1 0.2 copy.74
  11.4 0.2 copy.73
  11.6 0.1 fusion.22
  11.8 0.6 slice.233
  12.3 0.6 convert.9
  12.9 0.6 fusion.68
  13.6 1.9 rev.21
  15.5 0.1 convert_multiply_fusion.1
  15.6 1.9 rev.22
  17.5 0.2 copy_dynamic-update-slice_fusion.1
  17.8 0.2 copy.71
  18.0 3.9 %rev.19 = f32[768,128]{1,0:T(8,128)} reverse(f32[768,128]{1,0:T(8,128)} %get-tuple-element.12), dimensions={0} | reverse | bytes 786432 | tf_op jit(solution)/shard_map/jit(_flip)/rev | solution.py:442
  21.9 2.0 copy.72
  24.0 1.3 exponential_bitcast_fusion
  25.2 1.3 slice_bitcast_fusion.7
  26.5 1.5 copy.90
  28.0 0.2 copy_dynamic-update-slice_fusion
  28.3 2.6 %fusion.27 = (bf16[2,12,64,128]{3,1,2,0:T(8,128)(2,1)}, bf16[2,12,64,128]{3,1,2,0:T(8,128)(2,1)}, bf16[2,12,64,128]{3,1,2,0:T(8,128)(2,1)S(1)}) fusion(f32[2,12,64,128]{3,1,2,0:T(8,128)S(1)} %copy_dynamic-update-slice_fusion, f32[2,12,64,1,128]{4,1,2,3,0:T(8,128)S(1)} %fusion.22, f32[2,12,128]{2,1,0:T(8,128)} %get-tuple-element.6, ...), kind=kLoop, calls=%fused_computation.27 | loop fusion | flops 1769472 | bytes 3551232 | tf_op jit(solution)/shard_map/mul | solution.py:479
  30.9 0.8 copy-done.1
  31.7 0.4 fusion.45
  32.2 0.9 copy-done.10
  33.1 0.6 fusion
  33.8 0.9 broadcast_in_dim.113
  34.7 7.4 %all-to-all-start.1 = ((bf16[16,129,128]{2,1,0:T(8,128)(2,1)}), bf16[16,129,128]{2,1,0:T(8,128)(2,1)S(1)}, u32[]{:S(2)}, u32[]{:S(2)}) async-start(bf16[16,129,128]{2,1,0:T(8,128)(2,1)} %broadcast_in_dim.113), calls=%async_computation.1 | async-start | bytes 1114112 | tf_op jit(solution)/shard_map/all_to_all | solution.py:23
  42.2 0.1 copy.76
  42.3 0.1 copy.79
  42.4 0.1 copy.77
  42.6 2.4 %fusion.21 = f32[2,12,128,64]{2,3,1,0:T(8,128)} fusion(bf16[1,12,64,1,128]{4,2,1,0,3:T(8,128)(2,1)S(1)} %bitcast.116, bf16[1,12,64,1,128]{4,2,1,0,3:T(8,128)(2,1)S(1)} %bitcast.114, bf16[2,12,64,128]{3,1,2,0:T(8,128)(2,1)} %get-tuple-element.3, bf16[2,12,64,128]{3,1,2,0:T(8,128)(2,1)S(1)} %copy-done.2, pred[64,64]{1,0:T(8,128)(4,1)S(1)} %iota_compare_fusion), kind=kOutput, calls=%fused_computation.16 | convolution fusion | flops 50626560 | bytes 1970176 | tf_op jit(solution)/shard_map/nbhts,nbshv->nbthv/dot_general | solution.py:455
  45.0 6.3 %all-to-all-done.1 = bf16[16,129,128]{2,1,0:T(8,128)(2,1)S(1)} async-done(((bf16[16,129,128]{2,1,0:T(8,128)(2,1)}), bf16[16,129,128]{2,1,0:T(8,128)(2,1)S(1)}, u32[]{:S(2)}, u32[]{:S(2)}) %all-to-all-start.1) | async-done | bytes 528416 | tf_op jit(solution)/shard_map/all_to_all | solution.py:23
  51.4 0.9 broadcast_in_dim.108
  52.3 6.1 %all-to-all-start = ((bf16[16,129,128]{2,1,0:T(8,128)(2,1)}), bf16[16,129,128]{2,1,0:T(8,128)(2,1)S(1)}, u32[]{:S(2)}, u32[]{:S(2)}) async-start(bf16[16,129,128]{2,1,0:T(8,128)(2,1)} %broadcast_in_dim.108), calls=%async_computation | async-start | bytes 1114112 | tf_op jit(solution)/shard_map/all_to_all | solution.py:23
  58.3 0.2 all-gather.2.cloned.1.call-start
  58.6 0.1 broadcast_select_fusion
  58.7 0.1 select_bitcast_fusion
  59.0 7.6 %all-to-all-done = bf16[16,129,128]{2,1,0:T(8,128)(2,1)S(1)} async-done(((bf16[16,129,128]{2,1,0:T(8,128)(2,1)}), bf16[16,129,128]{2,1,0:T(8,128)(2,1)S(1)}, u32[]{:S(2)}, u32[]{:S(2)}) %all-to-all-start) | async-done | bytes 528416 | tf_op jit(solution)/shard_map/all_to_all | solution.py:23
  66.6 0.1 broadcast_select_fusion.1
  66.7 0.2 reverse_add_fusion
  66.9 0.1 slice_add_fusion.1
  67.1 0.1 slice_add_fusion.3
  67.2 0.1 slice_add_fusion.5
  67.3 0.1 select_bitcast_fusion.1
  67.4 0.2 slice_add_fusion
  67.6 0.1 slice_add_fusion.2
  67.8 0.1 slice_add_fusion.4
  68.0 0.4 copy-done.11
  68.4 2.8 %fusion.4 = bf16[2,12,128,128]{3,1,2,0:T(8,128)(2,1)S(1)} fusion(bf16[2,12,128,128]{3,2,1,0:T(8,128)(2,1)S(1)} %copy-done.11, f32[2,128,128]{2,1,0:T(8,128)S(1)} %maximum_bitcast_fusion.2, f32[2,12,128]{1,2,0:T(8,128)S(1)} %copy.79, f32[2,12,128]{1,2,0:T(8,128)S(1)} %copy.77, f32[2,12,128]{1,2,0:T(8,128)S(1)} %copy.76, pred[12,12]{1,0:T(8,128)(4,1)S(1)} %iota_compare_fusion.2), kind=kOutput, calls=%fused_computation.6 | convolution fusion | flops 10727424 | bytes 1740944 | tf_op jit(solution)/shard_map/nbchk,nchkv->nbhkv/dot_general | solution.py:464
  71.2 0.3 fusion.18
  71.7 0.2 rev.23
  71.9 0.2 multiply_reduce_fusion
  72.1 0.4 copy-done.16
  72.5 0.9 fusion.65
  73.4 0.2 copy.87
  73.6 0.2 copy.86
  73.9 0.2 fusion.88
  74.0 0.7 copy.89.eid_row
  74.9 0.9 broadcast_add_fusion.eid_col
  75.8 0.9 broadcast_multiply_fusion.weight_col
  76.7 123.0 %expert_side.1 = bf16[768,128]{1,0:T(8,128)(2,1)} custom-call(bf16[768,2048]{1,0:T(8,128)(2,1)} %x_hbm.1, f32[1,2048]{1,0:T(1,128)} %bitcast.126, s32[2,768]{1,0:T(2,128)} %copy.89.eid_row, s32[768,2]{1,0:T(8,128)} %broadcast_add_fusion.eid_col, f32[768,2]{1,0:T(8,128)} %broadcast_multiply_fusion.weight_col, bf16[2,2048,256]{2,1,0:T(8,128)(2,1)} %wg_hbm.1, ...), custom_call_target="tpu_custom_call" | custom-call | flops 40000000000 | bytes 20000000 | tf_op jit(solution)/shard_map/expert_side/pallas_call | solution.py:375
  199.7 3.6 %convolution_convert_fusion = bf16[768,128]{1,0:T(8,128)(2,1)} fusion(bf16[768,2048]{1,0:T(8,128)(2,1)} %all-gather.2.cloned.1.call-done, bf16[2048,128]{1,0:T(8,128)(2,1)S(1)} %copy-done), kind=kOutput, calls=%fused_computation.17 | convolution fusion | flops 402751488 | bytes 3866624 | tf_op jit(solution)/shard_map/dot_general | solution.py:489
  203.3 0.7 copy.118
  (79 shorter events, 0.7 us)
Async XLA Ops:
  7.2 192.6 %copy-start = (bf16[2048,128]{1,0:T(8,128)(2,1)S(1)}, bf16[2048,128]{1,0:T(8,128)(2,1)}, u32[]{:S(2)}) copy-start(bf16[2048,128]{1,0:T(8,128)(2,1)} %param.24) | copy-start | bytes 1572868
  11.1 2.5 %copy-start.5 = (bf16[768,128]{1,0:T(8,128)(2,1)S(1)}, bf16[768,128]{1,0:T(8,128)(2,1)}, u32[]{:S(2)}) copy-start(bf16[768,128]{1,0:T(8,128)(2,1)} %param.18) | copy-start | bytes 589828
  11.1 4.4 %copy-start.15 = (bf16[768,128]{1,0:T(8,128)(2,1)S(1)}, bf16[768,128]{1,0:T(8,128)(2,1)}, u32[]{:S(2)}) copy-start(bf16[768,128]{1,0:T(8,128)(2,1)} %param.17) | copy-start | bytes 589828
  18.0 10.0 %copy-start.4 = (f32[768,128]{1,0:T(8,128)S(1)}, f32[768,128]{1,0:T(8,128)}, u32[]{:S(2)}) copy-start(f32[768,128]{1,0:T(8,128)} %rev.22) | copy-start | bytes 1179652
  28.3 3.5 %copy-start.6 = (bf16[768,128]{1,0:T(8,128)(2,1)S(1)}, bf16[768,128]{1,0:T(8,128)(2,1)}, u32[]{:S(2)}) copy-start(bf16[768,128]{1,0:T(8,128)(2,1)} %param.18) | copy-start | bytes 589828
  28.3 3.5 %copy-start.8 = (bf16[768,128]{1,0:T(8,128)(2,1)S(1)}, bf16[768,128]{1,0:T(8,128)(2,1)}, u32[]{:S(2)}) copy-start(bf16[768,128]{1,0:T(8,128)(2,1)} %rev.21) | copy-start | bytes 589828
  28.3 4.8 %copy-start.17 = (bf16[2,12,128,1]{1,3,2,0:T(2,128)(2,1)S(1)}, bf16[2,12,128,1]{1,3,2,0:T(2,128)(2,1)}, u32[]{:S(2)}) copy-start(bf16[2,12,128,1]{1,3,2,0:T(2,128)(2,1)} %copy.90) | copy-start | bytes 18436
  30.9 0.8 copy-start.1
  30.9 2.9 %copy-start.23 = (bf16[1,128]{1,0:T(2,128)(2,1)S(1)}, bf16[1,128]{1,0:T(2,128)(2,1)}, u32[]{:S(2)}) copy-start(bf16[1,128]{1,0:T(2,128)(2,1)} %get-tuple-element.22) | copy-start | bytes 772
  32.2 0.9 copy-start.10
  33.1 9.1 %copy-start.18 = (f32[2,12,128]{2,1,0:T(8,128)S(1)}, f32[2,12,128]{2,1,0:T(8,128)}, u32[]{:S(2)}) copy-start(f32[2,12,128]{2,1,0:T(8,128)} %get-tuple-element.5) | copy-start | bytes 36868
  33.1 9.5 %copy-start.22 = (bf16[1,128]{1,0:T(2,128)(2,1)S(1)}, bf16[1,128]{1,0:T(2,128)(2,1)}, u32[]{:S(2)}) copy-start(bf16[1,128]{1,0:T(2,128)(2,1)} %get-tuple-element.21) | copy-start | bytes 772
  33.1 9.5 %copy-start.2 = (bf16[2,12,64,128]{3,1,2,0:T(8,128)(2,1)S(1)}, bf16[2,12,64,128]{3,1,2,0:T(8,128)(2,1)}, u32[]{:S(2)}) copy-start(bf16[2,12,64,128]{3,1,2,0:T(8,128)(2,1)} %copy-done.1) | copy-start | bytes 1179652
  33.1 9.5 %copy-start.7 = (bf16[768,128]{1,0:T(8,128)(2,1)S(1)}, bf16[768,128]{1,0:T(8,128)(2,1)}, u32[]{:S(2)}) copy-start(bf16[768,128]{1,0:T(8,128)(2,1)} %param.18) | copy-start | bytes 589828
  33.1 9.5 %copy-start.9 = (bf16[768,128]{1,0:T(8,128)(2,1)S(1)}, bf16[768,128]{1,0:T(8,128)(2,1)}, u32[]{:S(2)}) copy-start(bf16[768,128]{1,0:T(8,128)(2,1)} %rev.21) | copy-start | bytes 589828
  34.7 16.7 %all-to-all-start.1 = ((bf16[16,129,128]{2,1,0:T(8,128)(2,1)}), bf16[16,129,128]{2,1,0:T(8,128)(2,1)S(1)}, u32[]{:S(2)}, u32[]{:S(2)}) async-start(bf16[16,129,128]{2,1,0:T(8,128)(2,1)} %broadcast_in_dim.113), calls=%async_computation.1 | async-start | bytes 1114112 | tf_op jit(solution)/shard_map/all_to_all | solution.py:23
  52.3 14.3 %all-to-all-start = ((bf16[16,129,128]{2,1,0:T(8,128)(2,1)}), bf16[16,129,128]{2,1,0:T(8,128)(2,1)S(1)}, u32[]{:S(2)}, u32[]{:S(2)}) async-start(bf16[16,129,128]{2,1,0:T(8,128)(2,1)} %broadcast_in_dim.108), calls=%async_computation | async-start | bytes 1114112 | tf_op jit(solution)/shard_map/all_to_all | solution.py:23
  58.3 141.4 %all-gather.2.cloned.1.call-start = ((), (), s32[]{:S(2)}) async-start(), calls=%async_computation.2 | async-start | bytes 3342336 | tf_op jit(solution)/shard_map/all_gather | solution.py:490
  67.3 1.1 copy-start.11
  68.4 2.8 %copy-start.3 = (bf16[2,12,64,128]{3,1,2,0:T(8,128)(2,1)S(1)}, bf16[2,12,64,128]{3,1,2,0:T(8,128)(2,1)}, u32[]{:S(2)}) copy-start(bf16[2,12,64,128]{3,1,2,0:T(8,128)(2,1)} %get-tuple-element.2) | copy-start | bytes 1179652
  68.4 2.8 %copy-start.12 = (f32[2,12,128,64]{2,3,1,0:T(8,128)S(1)}, f32[2,12,128,64]{2,3,1,0:T(8,128)}, u32[]{:S(2)}) copy-start(f32[2,12,128,64]{2,3,1,0:T(8,128)} %fusion.21) | copy-start | bytes 2359300
  71.6 0.9 copy-start.16
  71.6 0.9 copy-start.24
  71.6 1.8 copy-start.20
  71.6 2.0 copy-start.21
  71.7 2.2 %copy-start.19 = (s32[768]{0:T(1024)S(1)}, s32[768]{0:T(1024)}, u32[]{:S(2)}) copy-start(s32[768]{0:T(1024)} %param.27) | copy-start | bytes 9220
  71.9 2.9 %copy-start.13 = (f32[768,8]{0,1:T(8,128)S(1)}, f32[768,8]{0,1:T(8,128)}, u32[]{:S(2)}) copy-start(f32[768,8]{0,1:T(8,128)} %param.29) | copy-start | bytes 73732
  199.7 3.6 %copy-start.14 = (bf16[768,128]{1,0:T(8,128)(2,1)S(1)}, bf16[768,128]{1,0:T(8,128)(2,1)}, u32[]{:S(2)}) copy-start(bf16[768,128]{1,0:T(8,128)(2,1)} %expert_side.1) | copy-start | bytes 589828
Sparse Core Ops, SparseCore 0:
  73.5 48.0 all-gather.1

commit v2 on v1

v2 whole, which is shorter than its diff:
```python
import jax
import jax.numpy as jnp
from jax import lax
from jax.experimental import pallas as pl
from jax.experimental.pallas import tpu as pltpu
from jax.sharding import Mesh
from jax.sharding import PartitionSpec as P

GROUP_EXP = 4
BLOCK = 64
TP = ("tp_0", "tp_1")


HEAD_EPS = 1e-06
NORM_EPS = 1e-05


F32, BF16 = jnp.float32, jnp.bfloat16
RINGS = ((0, 0), (0, 1), (1, 0), (1, 1))


def mm(a, b):
    return jnp.dot(a, b, preferred_element_type=F32)


def dot_last(a, b):
    return lax.dot_general(a, b, (((1,), (1,)), ((), ())), preferred_element_type=F32)


def thirds(value):
    high = value.astype(BF16)
    rest = value - high.astype(F32)
    middle = rest.astype(BF16)
    return high, middle, (rest - middle.astype(F32)).astype(BF16)


def whole_kernel(
    x_hbm, gain, group_index, pair, group_scores, pair_scores, wg_hbm, wu_hbm, wd_hbm,
    queries, values, logits, gates, headroom, spike, head_gain, proj_hbm,
    rec_out, out,
    x, normed, wg, wu, wd, rank_row, send_buf, arrived, partial, pair_buf,
    ring_buf, final_buf, ret, pick0, pick1,
    proj, cum, joined, block_state, block_total, entry_state, entry_sum, decayed,
    state_send, states, incoming, readout, columns,
    load_sem, disp_send, disp_recv, fwd_send, fwd_recv, pair_send, pair_recv,
    ring_send, ring_recv, ret_send, ret_recv,
    state_ssem, state_rsem, read_send, read_recv, side_send, side_recv,
):
    side = arrived.shape[1]
    cap = arrived.shape[3]
    zs = partial.shape[1]
    rows, width = x.shape
    group_rows = side * cap
    ep_size = side * side
    experts = 2 * ep_size
    me, z, core = lax.axis_index("ep"), lax.axis_index("tp_0"), lax.axis_index("tp_1")
    my_y, my_x = me // side, me % side
    loads = [
        pltpu.make_async_copy(a, b, load_sem.at[n])
        for n, (a, b) in enumerate((
            (x_hbm, x), (wg_hbm, wg), (wu_hbm, wu), (wd_hbm, wd), (proj_hbm, proj)
        ))
    ]
    loads[0].start()

    barrier = pltpu.get_barrier_semaphore()

    def greet(n, carry):
        pl.semaphore_signal(barrier, 1, device_id={"ep": (me + n) % ep_size})
        return carry

    lax.fori_loop(1, ep_size, greet, 0)
    pl.semaphore_signal(barrier, 1, device_id={"tp_1": 1 - core})
    pl.semaphore_signal(barrier, 1, device_id={"tp_0": (z + 1) % zs})
    pl.semaphore_signal(barrier, 1, device_id={"tp_0": (z + zs - 1) % zs})

    def target(k, m):
        return ((my_y + 2 * side - (m + k) % side) % side) * side + (my_x + side - m) % side

    def source(k, m):
        return ((my_y + (m + k) % side) % side) * side + (my_x + m) % side

    first = lax.broadcasted_iota(jnp.int32, (rows, rows), 0)
    second = lax.broadcasted_iota(jnp.int32, (rows, rows), 1)
    ids = lax.broadcasted_iota(jnp.int32, (experts, rows), 0)
    group = group_index[...].reshape(1, rows)
    chosen = [ids == group * GROUP_EXP + pair[n : n + 1, :] for n in range(2)]
    named = chosen[0] | chosen[1]
    before = jnp.where(first < second, 1.0, 0.0).astype(BF16)
    rank = mm(jnp.where(named, 1.0, 0.0).astype(BF16), before)
    rank_row[...] = jnp.where(named, rank, -1.0)
    away_y = (my_y + side - ids // (2 * side)) % side
    away_x = (my_x + side - ids // 2 % side) % side
    step_of = (away_y + side - away_x) % side
    slot = rank + (cap * ((step_of * side + away_x) * 2 + ids % 2)).astype(F32)
    powers = jnp.exp(group_scores[...] - jnp.max(group_scores[...], axis=0, keepdims=True))
    groups = lax.broadcasted_iota(jnp.int32, powers.shape, 0)
    share = jnp.sum(jnp.where(groups == group, powers, 0.0), axis=0, keepdims=True) / jnp.sum(
        powers, axis=0, keepdims=True
    )
    lead = pair_scores[0:1, :] - pair_scores[1:2, :]
    lines = [jnp.sum(jnp.where(which, slot, 0.0), axis=0, keepdims=True) for which in chosen]
    lines += [share * jax.nn.sigmoid(lead), share * jax.nn.sigmoid(-lead), spike[...].reshape(1, rows)]
    columns[...] = jnp.concatenate(lines + [jnp.zeros((3, rows), F32)], 0).T
    wide = 4 * BLOCK
    blocks = rows // BLOCK
    at_row = lax.broadcasted_iota(jnp.int32, (wide, wide), 0)
    at_col = lax.broadcasted_iota(jnp.int32, (wide, wide), 1)
    same = at_row // BLOCK == at_col // BLOCK
    reach = (same & (at_col <= at_row), same & (at_col >= at_row))
    block_of = lax.broadcasted_iota(jnp.int32, (wide, 128), 0) // BLOCK

    def local_part(g, carry):
        at = pl.ds(pl.multiple_of(g * wide, wide), wide)
        lifted = jax.nn.silu(queries[at, :].astype(F32))
        inputs = values[at, :]
        inputs_t = inputs.astype(F32).T.astype(BF16)
        scores = jnp.zeros((wide, wide), F32)
        for d in range(2):
            keys = headroom[d : d + 1, :] * jax.nn.sigmoid(-logits[d, at, :].astype(F32))
            decay = jnp.log1p(-keys) + columns[at, 4:5]
            sums = mm(
                jnp.where(reach[d], 1.0, 0.0).astype(BF16), jnp.concatenate(thirds(decay), 1)
            )
            run = sums[:, :128] + sums[:, 128:256] + sums[:, 256:]
            cum[d, at, :] = run
            run4 = run.reshape(4, BLOCK, 128)
            middle = run4[:, BLOCK // 2 : BLOCK // 2 + 1]
            last = run4[:, BLOCK - 1 :] if d == 0 else run4[:, :1]
            over = (run4 - middle).reshape(wide, 128)
            left = (last - run4).reshape(wide, 128)
            found = dot_last(
                (lifted * jnp.exp(over)).astype(BF16), (keys * jnp.exp(-over)).astype(BF16)
            )
            scores = scores + jnp.where(reach[d], found, 0.0)
            written = keys * jnp.exp(left)
            spread = jnp.concatenate(
                [jnp.where(block_of == b, written, 0.0).astype(BF16) for b in range(4)], 1
            )
            state = mm(inputs_t, spread)
            for b in range(4):
                block_state[d, 4 * g + b] = state[:, 128 * b : 128 * b + 128]
                block_total[d, 4 * g + b] = last[b]
            decayed[at, 128 * d : 128 * d + 128] = (lifted * jnp.exp(run)).astype(BF16)
        joined[at, :] = mm(scores.astype(BF16), inputs)
        return carry

    lax.fori_loop(0, rows // wide, local_part, 0)

    line = lax.broadcasted_iota(jnp.int32, (16, 128), 0)
    for d in range(2):
        def advance(n, carry, d=d):
            state, total = carry
            b = n if d == 0 else blocks - 1 - n
            entry_state[b, :, 128 * d : 128 * d + 128] = state.astype(BF16)
            entry_sum[d, b] = total
            own = block_total[d, b]
            return jnp.exp(own) * state + block_state[d, b], total + own

        state, total = lax.fori_loop(
            0, blocks, advance, (jnp.zeros((128, 128), F32), jnp.zeros((1, 128), F32))
        )
        state_send[d, :128] = state.astype(BF16)
        terms = jnp.zeros((16, 128), F32)
        for n, term in enumerate(thirds(total)):
            terms = jnp.where(line == n, term.astype(F32), terms)
        state_send[d, 128:] = terms.astype(BF16)

    pl.semaphore_wait(barrier, ep_size + 2)

    def state_copy(n):
        there = (me + n) % ep_size
        return pltpu.make_async_remote_copy(
            state_send.at[1 - (there + ep_size - me) // ep_size], states.at[me],
            state_ssem.at[n], state_rsem.at[me], device_id={"ep": there},
        )

    def state_start(n, carry):
        state_copy(n).start()
        return carry

    lax.fori_loop(1, ep_size, state_start, 0)

    def state_sent(n, carry):
        state_copy(n).wait_send()
        return carry

    loads[0].wait()
    for load in loads[1:]:
        load.start()
    step_rows = rows // 8

    def norm_step(n, carry):
        at = pl.ds(pl.multiple_of(n * step_rows, step_rows), step_rows)
        features = x[at, :].astype(F32)
        centred = features - jnp.mean(features, -1, keepdims=True)
        spread = lax.rsqrt(jnp.mean(centred * centred, -1, keepdims=True) + NORM_EPS)
        normed[at, :] = (centred * spread * gain[...]).astype(BF16)
        return carry

    lax.fori_loop(0, rows // step_rows, norm_step, 0)

    def dispatch_copy(k, m):
        return pltpu.make_async_remote_copy(
            send_buf.at[k, m], arrived.at[core, k, m], disp_send.at[k, m], disp_recv.at[k, m],
            device_id={"ep": target(k, m)},
        )

    def forward_copy(k, m):
        return pltpu.make_async_remote_copy(
            arrived.at[core, k, m], arrived.at[core, k, m], fwd_send.at[k, m], fwd_recv.at[k, m],
            device_id={"tp_1": 1 - core},
        )

    def dispatch_start(k, m, n):
        lanes = slice(n * width // 2, (n + 1) * width // 2)
        pltpu.make_async_remote_copy(
            send_buf.at[k, m, :, lanes], arrived.at[core, k, m, :, lanes],
            disp_send.at[k, m], disp_recv.at[k, m], device_id={"ep": target(k, m)},
        ).start()

    def dispatch_group(k):
        for n in range(2):
            for m in range(side):
                if m == 0:
                    pl.when(k > 0)(lambda n=n: dispatch_start(k, 0, n))
                else:
                    dispatch_start(k, m, n)

    places_row = lax.broadcasted_iota(jnp.int32, (cap, rows), 0).astype(F32)

    def selection(k):
        picks = [
            jnp.where(
                rank_row[pl.ds(2 * target(k, m) + core, 1), :] == places_row, 1.0, 0.0
            ).astype(BF16)
            for m in range(side)
        ]
        return jnp.concatenate(picks, 0)

    def gather_group(k):
        sel = selection(k)
        for n in range(2):
            for at in range(n * width // 2, (n + 1) * width // 2, 512):
                got = mm(sel, normed[:, at : at + 512]).astype(BF16)
                send_buf[k, :, :, at : at + 512] = got.reshape(side, cap, 512)

        @pl.when(k == 0)
        def _():
            arrived[core, 0, 0] = send_buf[0, 0]

        pl.when(k < 2)(lambda: dispatch_group(k))

    lax.fori_loop(1, ep_size, state_sent, 0)

    def gather_whole(k, carry):
        gather_group(k)
        return carry

    lax.fori_loop(0, side, gather_whole, 0)

    def across(b, carry):
        at = pl.ds(pl.multiple_of(b * BLOCK, BLOCK), BLOCK)
        joined[at, :] += dot_last(decayed[at, :], entry_state[b])
        lifted = jax.nn.silu(queries[at, :].astype(F32))
        for d in range(2):
            decayed[at, 128 * d : 128 * d + 128] = (
                lifted * jnp.exp(cum[d, at, :] + entry_sum[d, b])
            ).astype(BF16)
        return carry

    lax.fori_loop(0, blocks, across, 0)

    places = lax.broadcasted_iota(jnp.int32, pick0.shape, 1).astype(F32)
    for n, pick in enumerate((pick0, pick1)):
        pick[...] = jnp.where(places == columns[:, n : n + 1], 1.0, 0.0).astype(BF16)

    for load in loads[1:]:
        load.wait()

    def read_slice(chip, which):
        return pl.ds(pl.multiple_of((2 * chip + which) * 128, 128), 128)

    def read_copy(f, s):
        chip = (z + zs - s) % zs if f == 0 else (z + s) % zs
        lines = pl.ds(0, rows) if s < zs // 2 - 1 else pl.ds(f * (rows // 2), rows // 2)
        piece = readout.at[lines, read_slice(chip, core)]
        return pltpu.make_async_remote_copy(
            piece, piece, read_send.at[f, s], read_recv.at[f, s],
            device_id={"tp_0": (z + 1) % zs if f == 0 else (z + zs - 1) % zs},
        )

    def side_copy(distance):
        piece = readout.at[:, read_slice((z + distance) % zs, core)]
        return pltpu.make_async_remote_copy(
            piece, piece, side_send.at[distance], side_recv.at[distance],
            device_id={"tp_1": 1 - core},
        )

    def read_step(s):
        for f in range(2):
            if s > 0:
                read_copy(f, s - 1).wait_recv()
            if s < zs // 2:
                read_copy(f, s).start()
        for distance in {s % zs, (zs - s) % zs}:
            side_copy(distance).start()

    def finish_readout():
        for d in range(2):
            lanes = slice(128 * d, 128 * d + 128)

            def one(n, state, d=d):
                source_at = n if d == 0 else ep_size - 1 - n
                used = source_at < me if d == 0 else source_at > me

                def taken(state):
                    pltpu.make_async_remote_copy(
                        state_send.at[0], states.at[source_at], state_ssem.at[0],
                        state_rsem.at[source_at], device_id={"ep": source_at},
                    ).wait_recv()
                    got = states[source_at].astype(F32)
                    total = jnp.sum(got[128:], axis=0, keepdims=True)
                    return jnp.exp(total) * state + got[:128]

                return lax.cond(used, taken, lambda state: state, state)

            state = lax.fori_loop(0, ep_size, one, jnp.zeros((128, 128), F32))
            incoming[:, lanes] = state.astype(BF16)

        def settle(g, carry):
            at = pl.ds(pl.multiple_of(g * wide, wide), wide)
            total = joined[at, :] + dot_last(decayed[at, :], incoming[...])
            scale = lax.rsqrt(jnp.mean(total * total, -1, keepdims=True) + HEAD_EPS)
            gate = jax.nn.silu(gates[at, :].astype(F32))
            readout[at, read_slice(z, core)] = (total * scale * head_gain[...] * gate).astype(BF16)
            return carry

        lax.fori_loop(0, rows // wide, settle, 0)
        read_step(0)

    def ring_length(h, f):
        return zs // 2 if h == f else zs // 2 - 1

    def half(h):
        return pl.ds(h * group_rows, group_rows)

    def neighbour(f):
        return (z + 1) % zs if f == 0 else (z + zs - 1) % zs

    def ring_copy(k, h, f, s):
        length = ring_length(h, f)
        toward = (z + length) % zs if f == 0 else (z + zs - length) % zs
        origin = partial.at[k, toward, core, half(h)] if s == 0 else ring_buf.at[k, h, f, s - 1]
        return pltpu.make_async_remote_copy(
            origin, ring_buf.at[k, h, f, s], ring_send.at[k, h, f, s], ring_recv.at[k, h, f, s],
            device_id={"tp_0": neighbour(f)},
        )

    def ring_step(k, s, only=None):
        for h, f in RINGS:
            length = ring_length(h, f)
            if s >= length or only not in (None, h):
                continue
            if s > 0:
                ring_copy(k, h, f, s - 1).wait_recv()
                left = length - s
                toward = (z + left) % zs if f == 0 else (z + zs - left) % zs
                ring_buf[k, h, f, s - 1] = (
                    ring_buf[k, h, f, s - 1].astype(F32)
                    + partial[k, toward, core, half(h)].astype(F32)
                ).astype(BF16)
            ring_copy(k, h, f, s).start()

    def pair_copy(k, q):
        return pltpu.make_async_remote_copy(
            partial.at[k, :, 1 - core, half(q)], pair_buf.at[k, :, half(q)],
            pair_send.at[k, q], pair_recv.at[k, q], device_id={"tp_1": 1 - core},
        )

    def return_copy(k, m):
        return pltpu.make_async_remote_copy(
            final_buf.at[k, :, m], ret.at[k, m], ret_send.at[k, m], ret_recv.at[k, m],
            device_id={"ep": source(k, m)},
        )

    def finish(k):
        for h in range(2):
            lengths = [ring_length(h, f) for f in range(2)]
            for f in range(2):
                ring_copy(k, h, f, lengths[f] - 1).wait_recv()
            total = (
                partial[k, z, core, half(h)].astype(F32)
                + ring_buf[k, h, 0, lengths[0] - 1].astype(F32)
                + ring_buf[k, h, 1, lengths[1] - 1].astype(F32)
            )
            final_buf[k, h] = total.astype(BF16).reshape(final_buf.shape[2:])
        for m in range(side):
            if m == 0:
                @pl.when(k == 0)
                def _():
                    ret[0, 0] = final_buf[0, :, 0]

                @pl.when(k > 0)
                def _():
                    return_copy(k, m).start()
            else:
                return_copy(k, m).start()

    def take_pair(k, q):
        pair_copy(k, q).wait_recv()
        for d in range(zs):
            partial[k, d, core, half(q)] = (
                partial[k, d, core, half(q)].astype(F32) + pair_buf[k, d, half(q)].astype(F32)
            ).astype(BF16)
        ring_step(k, 0, q)

    def compute(k):
        for q in range(2):
            tokens = arrived[q, k].reshape(group_rows, width)
            gate = mm(tokens, wg[q])
            up = mm(tokens, wu[q])
            hidden = (jax.nn.silu(gate) * up).astype(BF16)
            for n in range(0, width, 512):
                part = mm(hidden, wd[q, :, n : n + 512]).astype(BF16)
                for i in range(4):
                    s = n // 128 + i
                    partial[k, s // 2, s % 2, half(q)] = part[:, 128 * i : 128 * i + 128]
            pair_copy(k, q).start()

    def group_step(k, carry):
        pl.when(k == 0)(lambda: read_step(1))
        for m in range(side):
            if m == 0:
                pl.when(k > 0)(lambda: dispatch_copy(k, 0).wait_send())
            else:
                dispatch_copy(k, m).wait_send()
        pl.when(k < side - 2)(lambda: dispatch_group(k + 2))
        for m in range(side):
            if m == 0:
                pl.when(k > 0)(lambda: dispatch_copy(k, 0).wait_recv())
            else:
                dispatch_copy(k, m).wait_recv()
            forward_copy(k, m).start()

        for n in range(1, side):
            pl.when(k >= n)(lambda n=n: ring_step(k - n, n))
        for m in range(side):
            forward_copy(k, m).wait_recv()
        compute(k)
        for q in range(2):
            take_pair(k, q)

        for n in range(2, side + 1):
            pl.when(k == n - 2)(lambda n=n: read_step(n))
        return carry

    finish_readout()
    lax.fori_loop(0, side, group_step, 0)
    final = side - 1
    ring_step(final, 1)
    ring_step(final - 1, 2)
    ring_step(final - 2, 3)
    finish(final - 3)
    ring_step(final, 2)
    ring_step(final - 1, 3)
    finish(final - 2)
    for distance in range(zs):
        side_copy(distance).wait_recv()
    rec_out[...] = mm(readout[...], proj[...])
    ring_step(final, 3)
    finish(final - 1)

    def take_returns(k, carry):
        for m in range(side):
            if m == 0:
                pl.when(k > 0)(lambda: return_copy(k, 0).wait_recv())
            else:
                return_copy(k, m).wait_recv()
        return carry

    def combined(k, count):
        copies = ret[k : k + count].reshape(count * 2 * group_rows, 128)
        lanes = slice(k * 2 * group_rows, (k + count) * 2 * group_rows)
        return columns[:, 2:3] * mm(pick0[:, lanes], copies) + columns[:, 3:4] * mm(
            pick1[:, lanes], copies
        )

    lax.fori_loop(0, final, take_returns, 0)
    out[...] = combined(0, final)
    finish(final)
    take_returns(final, 0)
    out[...] += combined(final, 1)

    def drain(k, carry):
        for m in range(side):
            def sent():
                return_copy(k, m).wait_send()

            if m == 0:
                pl.when(k > 0)(sent)
            else:
                sent()
            forward_copy(k, m).wait_send()
        for q in range(2):
            pair_copy(k, q).wait_send()
        for h, f in RINGS:
            for s in range(ring_length(h, f)):
                ring_copy(k, h, f, s).wait_send()
        return carry

    lax.fori_loop(0, side, drain, 0)

    for s in range(zs // 2):
        for f in range(2):
            read_copy(f, s).wait_send()
    for distance in range(zs):
        side_copy(distance).wait_send()


def on_device(
    queries,
    values,
    forget_gate_logits,
    output_gate_logits,
    forget_gate_headroom,
    spike_log_decay,
    head_norm_gain,
    output_projection,
    second_micro_input,
    expert_norm_gain,
    token_group_index,
    token_expert_pair,
    group_router_scores,
    expert_router_scores,
    expert_gate_weight,
    expert_up_weight,
    expert_down_weight,
):
    rows, width = second_micro_input.shape
    ep_size, zs = lax.axis_size("ep"), lax.axis_size("tp_0")
    side = int(round(ep_size**0.5))
    experts = 2 * ep_size
    cap = 2 * rows // experts
    group_rows = side * cap
    ring_slots = zs // 2
    blocks = rows // BLOCK
    dma = pltpu.SemaphoreType.DMA
    vmem = pl.BlockSpec(memory_space=pltpu.VMEM)
    hbm = pl.BlockSpec(memory_space=pl.ANY)
    result = jax.ShapeDtypeStruct((rows, 128), F32)
    results = pl.pallas_call(
        whole_kernel,
        out_shape=(result, result),
        in_specs=[hbm, vmem, vmem, vmem, vmem, vmem, hbm, hbm, hbm]
        + [vmem, vmem, vmem, vmem, vmem, vmem, vmem, hbm],
        out_specs=(vmem, vmem),
        scratch_shapes=[
            pltpu.VMEM((rows, width), BF16),
            pltpu.VMEM((rows, width), BF16),
            pltpu.VMEM(expert_gate_weight.shape, BF16),
            pltpu.VMEM(expert_up_weight.shape, BF16),
            pltpu.VMEM(expert_down_weight.shape, BF16),
            pltpu.VMEM((experts, rows), F32),
            pltpu.VMEM((side, side, cap, width), BF16),
            pltpu.VMEM((2, side, side, cap, width), BF16),
            pltpu.VMEM((side, zs, 2, 2 * group_rows, 128), BF16),
            pltpu.VMEM((side, zs, 2 * group_rows, 128), BF16),
            pltpu.VMEM((side, 2, 2, ring_slots, group_rows, 128), BF16),
            pltpu.VMEM((side, 2, side, cap, 128), BF16),
            pltpu.VMEM((side, side, 2, cap, 128), BF16),
            pltpu.VMEM((rows, experts * cap), BF16),
            pltpu.VMEM((rows, experts * cap), BF16),
            pltpu.VMEM(output_projection.shape, BF16),
            pltpu.VMEM((2, rows, 128), F32),
            pltpu.VMEM((rows, 128), F32),
            pltpu.VMEM((2, blocks, 128, 128), F32),
            pltpu.VMEM((2, blocks, 1, 128), F32),
            pltpu.VMEM((blocks, 128, 256), BF16),
            pltpu.VMEM((2, blocks, 1, 128), F32),
            pltpu.VMEM((rows, 256), BF16),
            pltpu.VMEM((2, 144, 128), BF16),
            pltpu.VMEM((ep_size, 144, 128), BF16),
            pltpu.VMEM((128, 256), BF16),
            pltpu.VMEM((rows, 256 * zs), BF16),
            pltpu.VMEM((rows, 8), F32),
            dma((5,)),
            dma((side, side)), dma((side, side)),
            dma((side, side)), dma((side, side)),
            dma((side, 2)), dma((side, 2)),
            dma((side, 2, 2, ring_slots)), dma((side, 2, 2, ring_slots)),
            dma((side, side)), dma((side, side)),
            dma((ep_size,)), dma((ep_size,)),
            dma((2, ring_slots)), dma((2, ring_slots)),
            dma((zs,)), dma((zs,)),
        ],
        compiler_params=pltpu.CompilerParams(
            collective_id=0, has_side_effects=True, vmem_limit_bytes=60 * 1024 * 1024
        ),
        name="whole",
    )(
        second_micro_input,
        expert_norm_gain[None, :],
        token_group_index,
        token_expert_pair.T,
        group_router_scores.T,
        expert_router_scores.T,
        expert_gate_weight,
        expert_up_weight,
        expert_down_weight,
        queries,
        values,
        forget_gate_logits,
        output_gate_logits,
        forget_gate_headroom,
        spike_log_decay,
        head_norm_gain[None, :],
        output_projection,
    )
    return tuple(result.astype(BF16) for result in results)


def solution(mesh):
    split = Mesh(mesh.devices.reshape(mesh.shape["ep"], 8, 2), ("ep", "tp_0", "tp_1"))
    placed = (
        P("ep", TP),
        P("ep", TP),
        P(None, "ep", TP),
        P("ep", TP),
        P(None, TP),
        P("ep"),
        P(TP),
        P(None, TP),
        P("ep", None),
        P(),
        P("ep"),
        P("ep", None),
        P("ep", None),
        P("ep", None),
        P("ep", None, TP),
        P("ep", None, TP),
        P("ep", TP, None),
    )
    return jax.shard_map(
        on_device,
        mesh=split,
        in_specs=placed,
        out_specs=(P("ep", TP), P("ep", TP)),
        check_vma=False,
    )
```

time: 212 us -> 101 us (0.48)
  Pallas kernels: 123 us -> 96.4 us
  local copies, waits for them, and re-layouts: 22.3 us -> 0 us
  between operations: 14.7 us -> 0.65 us
  waiting for transfers between devices: 14 us -> 0 us
  starting transfers between devices: 13.8 us -> 0 us
  matrix products: 10.2 us -> 0 us
  other arithmetic: 13 us -> 3.38 us
    pallas_call x1, Pallas kernels: 123 us -> 96.4 us  [on_device(): pl.pallas_call(whole_kernel, out_shape=(result, result), in_specs=[hbm, v...]
    all_to_all x2 -> x0, waiting for transfers between devices: 13.9 us -> none  [from_everyone(): return lax.all_to_all(copies, axis, split_axis=0, concat_axis=0, tiled=True)]
    all_to_all x2 -> x0, starting transfers between devices: 13.5 us -> none  [from_everyone(): return lax.all_to_all(copies, axis, split_axis=0, concat_axis=0, tiled=True)]
    dot_general x6 -> x0, matrix products: 10.2 us -> none  [the longest x1 3.59 us: on_device(): jnp.dot(lax.all_gather(readout, TP, axis=1, tiled=True), output_projectio...]
    rev x5 -> x0, local copies, waits for them, and re-layouts: 8.07 us -> none  [the longest x4 7.9 us: directed(): both = jnp.stack([tensor[0], jnp.flip(tensor[1], 0)])]
    mul x8 -> x0, other arithmetic: 5.78 us -> none  [the longest x1 2.59 us: on_device(): query_dir * jnp.exp(running_state)]
    unnamed x53 -> x0, local copies, waits for them, and re-layouts: 3.79 us -> none
    another operation x6 -> x0, local copies, waits for them, and re-layouts: 3.18 us -> none  [the longest x5 3 us: directed(): both = jnp.stack([tensor[0], jnp.flip(tensor[1], 0)])]
  transfers between devices with their start and end apart: 3 -> 0, of which waited for: 2 -> 0; matrix products, arithmetic and copies ran while one was open for 3% -> 0% of each run, Pallas kernels for 58% -> 0%
where the time goes in v2:
time: 101 us; the launch traced here: 100 us
  Pallas kernels  96.4 us (95%)
  other arithmetic  3.38 us (3%)
    pallas_call x1, Pallas kernels, on_device(): pl.pallas_call(whole_kernel, out_shape=(result, result), in_specs=[hbm, v...  96.4 us
    convert_element_type x2, other arithmetic, on_device(): return tuple((result.astype(BF16) for result in results))  3.38 us

profile of v2, /device:TPU:4, one launch (start us, length us, event | category | flops | bytes accessed | tf_op | source)
XLA Modules:
  0.0 100.5 jit_solution(3814718168096250275)
XLA Ops:
  0.6 96.4 %whole.1 = (f32[768,128]{1,0:T(8,128)}, f32[768,128]{1,0:T(8,128)}) custom-call(bf16[768,2048]{1,0:T(8,128)(2,1)} %x_hbm.1, f32[1,2048]{1,0:T(1,128)} %bitcast.6, s32[768]{0:T(1024)} %group_index.1, s32[2,768]{1,0:T(2,128)} %bitcast.7, f32[8,768]{1,0:T(8,128)} %bitcast.5, f32[2,768]{1,0:T(2,128)} %bitcast.8, bf16[2,2048,256]{2,1,0:T(8,128)(2,1)} %wg_hbm.1, ...), custom_call_target="tpu_custom_call" | custom-call | tf_op jit(solution)/shard_map/whole/pallas_call | solution.py:552
  97.1 1.7 %convert_element_type.6 = bf16[768,128]{1,0:T(8,128)(2,1)} convert(f32[768,128]{1,0:T(8,128)} %get-tuple-element.4) | non-fusion elementwise | flops 98304 | bytes 589824 | tf_op jit(solution)/shard_map/convert_element_type | solution.py:620
  98.8 1.7 %convert_element_type.7 = bf16[768,128]{1,0:T(8,128)(2,1)} convert(f32[768,128]{1,0:T(8,128)} %get-tuple-element.5) | non-fusion elementwise | flops 98304 | bytes 589824 | tf_op jit(solution)/shard_map/convert_element_type | solution.py:620
